TPU v7x, 256 devices: a 4x2x16 block of a 4x16x16 slice. The times are simulated.
256 devices in a mesh: grp: 2 (over y), fs: 16 (over z), tp: 8 (over x, core).
Axes of the slice: x: 4, y: 2, z: 16, core: 2. Of those that a mesh axis runs over, the one named last changes fastest.
The devices are a block of a 4x16x16 slice.
Arguments:
- stream_in: bfloat16 [12288, 2048], P(('grp', 'fs'), 'tp'), parts along dimension 0, may hold values from -6 to 6
- gain_before: bfloat16 [2048], P('tp'), may hold values from 0.099609375 to 1.8984375
- gain_mixer: bfloat16 [2048], P('tp'), may hold values from 0.099609375 to 1.8984375
- gain_after: bfloat16 [2048], P('tp'), may hold values from 0.099609375 to 1.8984375
- w_gate: bfloat16 [2048, 5632], P('fs', 'tp'), may hold values from -0.125 to 0.125
- w_upward: bfloat16 [2048, 5632], P('fs', 'tp'), may hold values from -0.125 to 0.125
- w_down: bfloat16 [5632, 2048], P('tp', 'fs'), may hold values from -0.078125 to 0.078125
- w_value: bfloat16 [2048, 1024], P('fs', 'tp'), may hold values from -0.125 to 0.125
- w_glu_gate: bfloat16 [2048, 1024], P('fs', 'tp'), may hold values from -0.125 to 0.125
- conv_taps: bfloat16 [31, 1024], P(None, 'tp'), may hold values from -1 to 1
- chan_gain: bfloat16 [1024], P('tp'), may hold values from 0.099609375 to 1.8984375
- chan_bias: bfloat16 [1024], P('tp'), may hold values from -3 to 3
- w_mix_out: bfloat16 [1024, 2048], P('tp', 'fs'), may hold values from -0.1875 to 0.1875
Outputs:
- stream_out: bfloat16 [12288, 2048], P(('grp', 'fs'), 'tp'), parts along dimension 0
There are 2 independent parts, one for each index of `grp`. A program takes and returns all parts, laid end to end along the dimension named above; an argument that names none is the same for every part. Nothing has to cross between parts.
All inputs are finite; a program needn't handle non-finite values.
Results may differ from a plain program's by a relative error of at most 0.017.
Values may be sent and summed in bfloat16 or wider, within the bound.
A program may use at most 64 MiB of HBM per device.

v0:
```python
import jax
import jax.numpy as jnp
from jax import lax
from jax.sharding import PartitionSpec as P

D = 2048
CHAN = 1024
KERNEL = 31
LEN = 128


epsilon = 1e-06


def from_everyone(x, axis):
    copies = jnp.broadcast_to(x, (lax.axis_size(axis), *x.shape))
    return lax.all_to_all(copies, axis, split_axis=0, concat_axis=0, tiled=True)


def over_copies(x, axis):
    return from_everyone(x, axis).sum(axis=0)


def laid_out(parts, dim):
    parts = jnp.moveaxis(parts, 0, dim)
    shape = parts.shape
    return parts.reshape(*shape[:dim], shape[dim] * shape[dim + 1], *shape[dim + 2 :])


def gathered_copies(x, axis, dim):
    return laid_out(from_everyone(x, axis), dim)


def in_blocks(x, dim, count):
    before, after = (x.shape[:dim], x.shape[dim + 1 :])
    return jnp.moveaxis(x.reshape(*before, count, -1, *after), dim, 0)


def sent_and_summed(x, axis, dim):
    parts = in_blocks(x, dim, lax.axis_size(axis))
    arrived = lax.all_to_all(parts, axis, split_axis=0, concat_axis=0, tiled=True)
    return arrived.astype(jnp.float32).sum(axis=0)


def in_one_piece(arrays, axis, dim, along):
    both = jnp.concatenate(arrays, axis=along)
    out, at, gathered = (lax.all_gather(both, axis, axis=dim, tiled=True), 0, [])
    for a in arrays:
        gathered.append(lax.slice_in_dim(out, at, at + a.shape[along], axis=along))
        at += a.shape[along]
    return tuple(gathered)


def normed_rows(stream, weights):
    values = stream.astype(jnp.float32)
    totals = over_copies(jnp.sum(values * values, axis=1), "tp")
    inverse = lax.rsqrt(totals / D + epsilon)
    scaled = (values * inverse[:, None] * weights.astype(jnp.float32)).astype(jnp.bfloat16)
    return gathered_copies(scaled, "tp", 1)


def settle(partial_term):
    return sent_and_summed(partial_term.astype(jnp.bfloat16), "tp", 1)


def pair_adder(rows, portions):
    return (
        jnp.dot(rows, portions[0], preferred_element_type=jnp.float32),
        jnp.dot(rows, portions[1], preferred_element_type=jnp.float32),
    )


def local(
    stream_in,
    gain_before,
    gain_mixer,
    gain_after,
    w_gate,
    w_upward,
    w_down,
    w_value,
    w_glu_gate,
    conv_taps,
    chan_gain,
    chan_bias,
    w_mix_out,
):
    whole_gate, whole_upward = in_one_piece((w_gate, w_upward), "fs", 0, 1)
    whole_down = lax.all_gather(w_down, "fs", axis=1, tiled=True)

    def feed_forward(rows):
        gate = jnp.dot(rows, whole_gate, preferred_element_type=jnp.float32)
        upward = jnp.dot(rows, whole_upward, preferred_element_type=jnp.float32)
        hidden = (jax.nn.silu(gate) * upward).astype(jnp.bfloat16)
        return settle(jnp.dot(hidden, whole_down, preferred_element_type=jnp.float32))

    first = (
        stream_in.astype(jnp.float32) + 0.5 * feed_forward(normed_rows(stream_in, gain_before))
    ).astype(jnp.bfloat16)
    rows = normed_rows(first, gain_mixer)
    value, gating = pair_adder(rows, in_one_piece((w_value, w_glu_gate), "fs", 0, 1))
    glued = value * jax.nn.sigmoid(gating)
    channels = glued.shape[1]
    grouped = glued.reshape(-1, LEN, channels)
    padded = jnp.pad(grouped, ((0, 0), (KERNEL - 1, 0), (0, 0)))
    taps = conv_taps.astype(jnp.float32)
    conv_sum = jnp.zeros_like(grouped)
    for lag_index in range(KERNEL):
        conv_sum = conv_sum + taps[lag_index] * padded[:, lag_index : lag_index + LEN]
    flat = conv_sum.reshape(-1, channels)
    sum_plain, sum_square = lax.psum((jnp.sum(flat, axis=1), jnp.sum(flat * flat, axis=1)), "tp")
    average = sum_plain / CHAN
    spread = sum_square / CHAN - average * average
    normed = (flat - average[:, None]) * lax.rsqrt(spread + epsilon)[:, None] * chan_gain.astype(
        jnp.float32
    ) + chan_bias.astype(jnp.float32)
    mixed = jax.nn.silu(normed).astype(jnp.bfloat16)
    branch = settle(
        jnp.dot(
            mixed,
            lax.all_gather(w_mix_out, "fs", axis=1, tiled=True),
            preferred_element_type=jnp.float32,
        )
    )
    second = (first.astype(jnp.float32) + branch).astype(jnp.bfloat16)
    third = second.astype(jnp.float32) + 0.5 * feed_forward(normed_rows(second, gain_after))
    return third.astype(jnp.bfloat16)


def solution(mesh):
    in_specs = (
        P(("grp", "fs"), "tp"),
        P("tp"),
        P("tp"),
        P("tp"),
        P("fs", "tp"),
        P("fs", "tp"),
        P("tp", "fs"),
        P("fs", "tp"),
        P("fs", "tp"),
        P(None, "tp"),
        P("tp"),
        P("tp"),
        P("tp", "fs"),
    )
    out_specs = P(("grp", "fs"), "tp")
    return jax.shard_map(local, mesh=mesh, in_specs=in_specs, out_specs=out_specs, check_vma=False)
```

profile of v0, /device:TPU:33, one launch (start us, length us, event | category | flops | bytes accessed | tf_op | source)
XLA Modules:
  0.0 407.0 jit_solution(14250651224693337071)
XLA Ops:
  6.6 1.8 pad_maximum_fusion
  10.9 23.7 %all-to-all-start = ((f32[8,1,384]{2,1,0:T(1,128)}), f32[8,1,384]{2,1,0:T(1,128)S(1)}, u32[]{:S(2)}, u32[]{:S(2)}) async-start(f32[8,1,384]{2,1,0:T(1,128)} %broadcast_in_dim.12), calls=%async_computation | async-start | bytes 24576 | tf_op jit(solution)/shard_map/all_to_all | solution.py:17
  35.3 4.0 all-to-all-done
  39.8 23.8 %all_to_all.48 = bf16[8,384,256]{1,2,0:T(8,128)(2,1)S(1)} all-to-all(bf16[8,384,256]{1,2,0:T(8,128)(2,1)S(1)} %broadcast_in_dim.13), channel_id=1, replica_groups=mesh['grp'=2,'fs'=16,'tp'=8] {'tp'}, dimensions={0} | all-to-all | bytes 3145728 | tf_op jit(solution)/shard_map/all_to_all | solution.py:17
  63.6 55.7 %all-gather.4.cloned.1.call-done = bf16[2048,1408]{0,1:T(8,128)(2,1)} async-done(((bf16[128,1408]{0,1:T(8,128)(2,1)}), bf16[2048,1408]{0,1:T(8,128)(2,1)}) %all-gather.4.cloned.1.call-update) | async-done | bytes 5767184 | tf_op jit(solution)/shard_map/all_gather | solution.py:47
  119.4 4.5 %fusion.4 = f32[384,704]{0,1:T(8,128)} fusion(bf16[384,2048]{0,1:T(8,128)(2,1)S(1)} %bitcast.120, bf16[2048,1408]{0,1:T(8,128)(2,1)} %all-gather.4.cloned.1.call-done), kind=kOutput, calls=%fused_computation.10 | convolution fusion | flops 1107296256 | bytes 5537792 | tf_op jit(solution)/shard_map/dot_general | solution.py:92
  123.9 75.0 %all-gather.6.cloned.1.call-done = bf16[704,2048]{1,0:T(8,128)(2,1)} async-done(((bf16[704,128]{1,0:T(8,128)(2,1)}), bf16[704,2048]{1,0:T(8,128)(2,1)}) %all-gather.6.cloned.1.call-update) | async-done | bytes 2883600 | tf_op jit(solution)/shard_map/all_gather | solution.py:89
  198.9 6.0 %convolution_convert_fusion.1 = bf16[384,2048]{1,0:T(8,128)(2,1)S(1)} fusion(bf16[704,2048]{1,0:T(8,128)(2,1)} %all-gather.6.cloned.1.call-done, bf16[384,2048]{0,1:T(8,128)(2,1)S(1)} %bitcast.121, bf16[2048,1408]{0,1:T(8,128)(2,1)} %all-gather.4.cloned.1.call-done, f32[384,704]{0,1:T(8,128)} %fusion.4), kind=kOutput, calls=%fused_computation.4 | convolution fusion | flops 2217000960 | bytes 9994240 | tf_op jit(solution)/shard_map/dot_general | solution.py:95
  206.3 15.6 %all-to-all-start.2 = ((bf16[8,384,256]{2,1,0:T(8,128)(2,1)}), bf16[8,384,256]{2,1,0:T(8,128)(2,1)S(1)}, u32[]{:S(2)}, u32[]{:S(2)}) async-start(bf16[8,384,256]{2,1,0:T(8,128)(2,1)} %bitcast.114), calls=%async_computation.2 | async-start | bytes 3145728 | tf_op jit(solution)/shard_map/all_to_all | solution.py:41
  222.6 19.8 %all-to-all-done.2 = bf16[8,384,256]{2,1,0:T(8,128)(2,1)S(1)} async-done(((bf16[8,384,256]{2,1,0:T(8,128)(2,1)}), bf16[8,384,256]{2,1,0:T(8,128)(2,1)S(1)}, u32[]{:S(2)}, u32[]{:S(2)}) %all-to-all-start.2) | async-done | bytes 1572896 | tf_op jit(solution)/shard_map/all_to_all | solution.py:41
  243.4 4.2 %all-to-all-start.3 = ((f32[8,1,384]{2,1,0:T(1,128)}), f32[8,1,384]{2,1,0:T(1,128)S(1)}, u32[]{:S(2)}, u32[]{:S(2)}) async-start(f32[8,1,384]{2,1,0:T(1,128)} %broadcast_in_dim.14), calls=%async_computation.3 | async-start | bytes 24576 | tf_op jit(solution)/shard_map/all_to_all | solution.py:17
  247.6 4.7 %all-to-all-done.3 = f32[8,1,384]{2,1,0:T(1,128)S(1)} async-done(((f32[8,1,384]{2,1,0:T(1,128)}), f32[8,1,384]{2,1,0:T(1,128)S(1)}, u32[]{:S(2)}, u32[]{:S(2)}) %all-to-all-start.3) | async-done | bytes 12320 | tf_op jit(solution)/shard_map/all_to_all | solution.py:17
  252.6 1.3 broadcast_in_dim.15
  254.0 4.3 %all-to-all-start.4 = ((bf16[8,384,256]{1,2,0:T(8,128)(2,1)}), bf16[8,384,256]{1,2,0:T(8,128)(2,1)S(1)}, u32[]{:S(2)}, u32[]{:S(2)}) async-start(bf16[8,384,256]{1,2,0:T(8,128)(2,1)} %broadcast_in_dim.15), calls=%async_computation.4 | async-start | bytes 3145728 | tf_op jit(solution)/shard_map/all_to_all | solution.py:17
  258.4 26.0 %all_gather.15 = bf16[128,2048]{1,0:T(8,128)(2,1)S(1)} all-gather(bf16[128,128]{1,0:T(8,128)(2,1)S(1)} %copy-done.1), channel_id=1, replica_groups=mesh['grp'=2,'fs'=16,'tp'=8] {'fs'}, dimensions={1}, use_global_device_ids=true | all-gather | bytes 557056 | tf_op jit(solution)/shard_map/all_gather | solution.py:121
  284.5 1.7 fusion.31
  287.6 18.3 %all-reduce.1 = (f32[384]{0:T(512)S(1)}, f32[384]{0:T(512)S(1)}) all-reduce(f32[384]{0:T(512)S(1)} %bitcast.128, f32[384]{0:T(512)S(1)} %bitcast.127), channel_id=1, replica_groups=mesh['grp'=2,'fs'=16,'tp'=8] {'tp'}, use_global_device_ids=true, to_apply=%region_8.9 | all-reduce | flops 768 | bytes 6144 | tf_op jit(solution)/shard_map/psum | solution.py:111
  306.8 23.7 %all_to_all.49 = bf16[8,384,256]{2,1,0:T(8,128)(2,1)S(1)} all-to-all(bf16[8,384,256]{2,1,0:T(8,128)(2,1)S(1)} %bitcast.116), channel_id=1, replica_groups=mesh['grp'=2,'fs'=16,'tp'=8] {'tp'}, dimensions={0} | all-to-all | bytes 3145728 | tf_op jit(solution)/shard_map/all_to_all | solution.py:41
  331.5 4.3 %all-to-all-start.6 = ((f32[8,1,384]{2,1,0:T(1,128)}), f32[8,1,384]{2,1,0:T(1,128)S(1)}, u32[]{:S(2)}, u32[]{:S(2)}) async-start(f32[8,1,384]{2,1,0:T(1,128)} %broadcast_in_dim.32), calls=%async_computation.6 | async-start | bytes 24576 | tf_op jit(solution)/shard_map/all_to_all | solution.py:17
  335.8 4.7 %all-to-all-done.6 = f32[8,1,384]{2,1,0:T(1,128)S(1)} async-done(((f32[8,1,384]{2,1,0:T(1,128)}), f32[8,1,384]{2,1,0:T(1,128)S(1)}, u32[]{:S(2)}, u32[]{:S(2)}) %all-to-all-start.6) | async-done | bytes 12320 | tf_op jit(solution)/shard_map/all_to_all | solution.py:17
  341.0 23.8 %all_to_all.50 = bf16[8,384,256]{1,2,0:T(8,128)(2,1)S(1)} all-to-all(bf16[8,384,256]{1,2,0:T(8,128)(2,1)S(1)} %broadcast_in_dim.33), channel_id=1, replica_groups=mesh['grp'=2,'fs'=16,'tp'=8] {'tp'}, dimensions={0} | all-to-all | bytes 3145728 | tf_op jit(solution)/shard_map/all_to_all | solution.py:17
  364.8 4.5 %fusion.6 = f32[384,704]{0,1:T(8,128)} fusion(bf16[384,2048]{0,1:T(8,128)(2,1)S(1)} %bitcast.122, bf16[2048,1408]{0,1:T(8,128)(2,1)} %all-gather.4.cloned.1.call-done), kind=kOutput, calls=%fused_computation.12 | convolution fusion | flops 1107296256 | bytes 5537792 | tf_op jit(solution)/shard_map/dot_general | solution.py:92
  369.3 6.0 %convolution_convert_fusion = bf16[384,2048]{1,0:T(8,128)(2,1)S(1)} fusion(bf16[704,2048]{1,0:T(8,128)(2,1)} %all-gather.6.cloned.1.call-done, bf16[384,2048]{0,1:T(8,128)(2,1)S(1)} %bitcast.123, bf16[2048,1408]{0,1:T(8,128)(2,1)} %all-gather.4.cloned.1.call-done, f32[384,704]{0,1:T(8,128)} %fusion.6), kind=kOutput, calls=%fused_computation.3 | convolution fusion | flops 2217000960 | bytes 9994240 | tf_op jit(solution)/shard_map/dot_general | solution.py:95
  375.4 24.1 %all_to_all.51 = bf16[8,384,256]{2,1,0:T(8,128)(2,1)S(1)} all-to-all(bf16[8,384,256]{2,1,0:T(8,128)(2,1)S(1)} %bitcast.117), channel_id=1, replica_groups=mesh['grp'=2,'fs'=16,'tp'=8] {'tp'}, dimensions={0} | all-to-all | bytes 3145728 | tf_op jit(solution)/shard_map/all_to_all | solution.py:41
  (69 shorter events, 11.8 us)
Async XLA Ops:
  6.5 32.8 %copy-start = (bf16[384,256]{1,0:T(8,128)(2,1)S(1)}, bf16[384,256]{1,0:T(8,128)(2,1)}, u32[]{:S(2)}) copy-start(bf16[384,256]{1,0:T(8,128)(2,1)} %param.13) | copy-start | bytes 589828
  6.5 112.8 %all-gather.4.cloned.1.call-start = ((), (), s32[]{:S(2)}) async-start(), calls=%async_computation.9 | async-start | bytes 6127616 | tf_op jit(solution)/shard_map/all_gather | solution.py:47
  8.4 190.5 %all-gather.6.cloned.1.call-start = ((), (), s32[]{:S(2)}) async-start(), calls=%async_computation.10 | async-start | bytes 3063808 | tf_op jit(solution)/shard_map/all_gather | solution.py:89
  10.9 28.4 %all-to-all-start = ((f32[8,1,384]{2,1,0:T(1,128)}), f32[8,1,384]{2,1,0:T(1,128)S(1)}, u32[]{:S(2)}, u32[]{:S(2)}) async-start(f32[8,1,384]{2,1,0:T(1,128)} %broadcast_in_dim.12), calls=%async_computation | async-start | bytes 24576 | tf_op jit(solution)/shard_map/all_to_all | solution.py:17
  206.3 15.6 %copy-start.2 = (bf16[128,128]{1,0:T(8,128)(2,1)S(1)}, bf16[128,128]{1,0:T(8,128)(2,1)}, u32[]{:S(2)}) copy-start(bf16[128,128]{1,0:T(8,128)(2,1)} %param.21) | copy-start | bytes 98308
  206.3 15.6 %copy-start.3 = (bf16[128,128]{1,0:T(8,128)(2,1)S(1)}, bf16[128,128]{1,0:T(8,128)(2,1)}, u32[]{:S(2)}) copy-start(bf16[128,128]{1,0:T(8,128)(2,1)} %param.20) | copy-start | bytes 98308
  206.3 36.2 %all-to-all-start.2 = ((bf16[8,384,256]{2,1,0:T(8,128)(2,1)}), bf16[8,384,256]{2,1,0:T(8,128)(2,1)S(1)}, u32[]{:S(2)}, u32[]{:S(2)}) async-start(bf16[8,384,256]{2,1,0:T(8,128)(2,1)} %bitcast.114), calls=%async_computation.2 | async-start | bytes 3145728 | tf_op jit(solution)/shard_map/all_to_all | solution.py:41
  221.9 25.7 %copy-start.6 = (bf16[256]{0:T(256)(128)(2,1)S(1)}, bf16[256]{0:T(256)(128)(2,1)}, u32[]{:S(2)}) copy-start(bf16[256]{0:T(256)(128)(2,1)} %param.15) | copy-start | bytes 1540
  221.9 62.6 %all-gather.8.cloned.1.call-start = ((), (), s32[]{:S(2)}) async-start(), calls=%async_computation.11 | async-start | bytes 1114112 | tf_op jit(solution)/shard_map/all_gather | solution.py:47
  243.4 8.9 %all-to-all-start.3 = ((f32[8,1,384]{2,1,0:T(1,128)}), f32[8,1,384]{2,1,0:T(1,128)S(1)}, u32[]{:S(2)}, u32[]{:S(2)}) async-start(f32[8,1,384]{2,1,0:T(1,128)} %broadcast_in_dim.14), calls=%async_computation.3 | async-start | bytes 24576 | tf_op jit(solution)/shard_map/all_to_all | solution.py:17
  254.0 4.4 %copy-start.4 = (bf16[31,128]{1,0:T(8,128)(2,1)S(1)}, bf16[31,128]{1,0:T(8,128)(2,1)}, u32[]{:S(2)}) copy-start(bf16[31,128]{1,0:T(8,128)(2,1)} %param.22) | copy-start | bytes 23812
  254.0 4.4 %copy-start.7 = (bf16[128]{0:T(256)(128)(2,1)S(1)}, bf16[128]{0:T(256)(128)(2,1)}, u32[]{:S(2)}) copy-start(bf16[128]{0:T(256)(128)(2,1)} %param.23) | copy-start | bytes 772
  254.0 4.4 %copy-start.8 = (bf16[128]{0:T(256)(128)(2,1)S(1)}, bf16[128]{0:T(256)(128)(2,1)}, u32[]{:S(2)}) copy-start(bf16[128]{0:T(256)(128)(2,1)} %param.24) | copy-start | bytes 772
  254.0 4.4 %copy-start.1 = (bf16[128,128]{1,0:T(8,128)(2,1)S(1)}, bf16[128,128]{1,0:T(8,128)(2,1)}, u32[]{:S(2)}) copy-start(bf16[128,128]{1,0:T(8,128)(2,1)} %param.25) | copy-start | bytes 98308
  254.0 30.5 %all-to-all-start.4 = ((bf16[8,384,256]{1,2,0:T(8,128)(2,1)}), bf16[8,384,256]{1,2,0:T(8,128)(2,1)S(1)}, u32[]{:S(2)}, u32[]{:S(2)}) async-start(bf16[8,384,256]{1,2,0:T(8,128)(2,1)} %broadcast_in_dim.15), calls=%async_computation.4 | async-start | bytes 3145728 | tf_op jit(solution)/shard_map/all_to_all | solution.py:17
  284.5 1.8 copy-start.5
  330.5 5.3 %copy-start.9 = (bf16[256]{0:T(256)(128)(2,1)S(1)}, bf16[256]{0:T(256)(128)(2,1)}, u32[]{:S(2)}) copy-start(bf16[256]{0:T(256)(128)(2,1)} %param.16) | copy-start | bytes 1540
  331.5 9.0 %all-to-all-start.6 = ((f32[8,1,384]{2,1,0:T(1,128)}), f32[8,1,384]{2,1,0:T(1,128)S(1)}, u32[]{:S(2)}, u32[]{:S(2)}) async-start(f32[8,1,384]{2,1,0:T(1,128)} %broadcast_in_dim.32), calls=%async_computation.6 | async-start | bytes 24576 | tf_op jit(solution)/shard_map/all_to_all | solution.py:17
Sparse Core Ops, SparseCore 0:
  9.1 110.2 all-gather.3
  121.1 77.7 all-gather.5
  224.5 55.1 all-gather.7
where the time goes:
time: 408 us; the launch traced here: 407 us
  waiting for transfers between devices  165 us (40%)
  blocking collectives  140 us (34%)
  starting transfers between devices  52.1 us (13%)
  matrix products  24 us (6%)
  between operations  13.4 us (3%)
  other arithmetic  7.32 us (2%)
  local copies, waits for them, and re-layouts  5.53 us (1%)
    all_gather x1, waiting for transfers between devices, local(): whole_down = lax.all_gather(w_down, 'fs', axis=1, tiled=True)  75 us
    all_gather x2, waiting for transfers between devices, in_one_piece(): lax.all_gather(both, axis, axis=dim, tiled=True)  55.7 us
    all_to_all x2, blocking collectives, sent_and_summed(): lax.all_to_all(parts, axis, split_axis=0, concat_axis=0, tiled=True)  47.8 us
    all_to_all x2, blocking collectives, from_everyone(): return lax.all_to_all(copies, axis, split_axis=0, concat_axis=0, tiled=True)  47.6 us
    all_to_all x4, starting transfers between devices, from_everyone(): return lax.all_to_all(copies, axis, split_axis=0, concat_axis=0, tiled=True)  36.5 us
    all_gather x1, blocking collectives, local(): lax.all_gather(w_mix_out, 'fs', axis=1, tiled=True)  26 us
    all_to_all x1, waiting for transfers between devices, sent_and_summed(): lax.all_to_all(parts, axis, split_axis=0, concat_axis=0, tiled=True)  19.8 us
    psum x1, blocking collectives, local(): lax.psum((jnp.sum(flat, axis=1), jnp.sum(flat * flat, axis=1)), 'tp')  18.3 us
  transfers between devices with their start and end apart: 8, of which 6 were waited for; matrix products, arithmetic and copies ran while one was open for 3% of the time, Pallas kernels for 0%

commit v1 on v0

v1 whole, which is shorter than its diff:
```python
import jax
import jax.numpy as jnp
from jax import lax
from jax.experimental import pallas as pl
from jax.experimental.pallas import tpu as pltpu
from jax.sharding import PartitionSpec as P

MESH = pl.DeviceIdType.MESH
LEN = 128
EPS = 1e-06
LANES = 128
CHUNKS = 3
BF16, F32 = jnp.bfloat16, jnp.float32

GU_X, WD_X, VM_X = 512, 208, 128


def remote(src, dst, send_sem, recv_sem, where):
    return pltpu.make_async_remote_copy(
        src_ref=src,
        dst_ref=dst,
        send_sem=send_sem,
        recv_sem=recv_sem,
        device_id=where,
        device_id_type=MESH,
    )


def layer_kernel(
    n_fs,
    n_tp,
    s_in,
    gu_in,
    wd_in,
    vm_in,
    pk_in,
    taps_in,
    out,
    gu,
    wd,
    vm,
    mxb,
    pk,
    gf,
    cgb,
    sb0,
    sb1,
    sb3,
    cvb,
    ub,
    mixed,
    hid,
    pad,
    sdo,
    sdi,
    acc,
    obo,
    obi,
    nbo,
    nbi,
    load_sem,
    z_recv,
    z_send,
    y_recv,
    y_send,
    pk_recv,
    pk_send,
    mx_recv,
    mx_send,
    ag_recv,
    ag_send,
    rs_recv,
    rs_send,
):
    z, t, g = lax.axis_index("fs"), lax.axis_index("tp"), lax.axis_index("grp")
    parity = lax.rem(g, 2)
    partner = {"grp": g + 1 - 2 * parity}
    z_right = {"fs": lax.rem(z + 1, n_fs)}
    z_left = {"fs": lax.rem(z + n_fs - 1, n_fs)}
    chips = n_tp // 2
    x, core = t // 2, lax.rem(t, 2)
    xr, xl, xo = lax.rem(x + 1, chips), lax.rem(x + 3, chips), lax.rem(x + 2, chips)
    other = 1 - core
    sib = {"tp": 2 * x + other}
    x_right, x_left = {"tp": 2 * xr + core}, {"tp": 2 * xl + core}

    nq, rows, width = sb0.shape[0], sb0.shape[1], s_in.shape[1]
    half = rows // 2
    feat = width * n_tp
    k_rows = gu_in.shape[0]
    chan_w = vm_in.shape[1] // 3
    chan = chan_w * n_tp
    steps = n_fs // 2

    def own_loads():
        yield pltpu.make_async_copy(gu_in, gu.at[pl.ds(pl.multiple_of(z * k_rows, k_rows), k_rows), :], load_sem.at[0])
        yield pltpu.make_async_copy(
            wd_in, wd.at[z // 2, :, pl.ds(pl.multiple_of(lax.rem(z, 2) * LANES, LANES), LANES)], load_sem.at[1]
        )
        yield pltpu.make_async_copy(vm_in, vm.at[pl.ds(pl.multiple_of(z * k_rows, k_rows), k_rows), :], load_sem.at[2])
        yield pltpu.make_async_copy(pk_in, pk.at[t], load_sem.at[3])
        for q in range(nq):
            yield pltpu.make_async_copy(
                s_in.at[pl.ds(q * rows, rows), :],
                sb0.at[q, :, pl.ds(pl.multiple_of(t * width, width), width)],
                load_sem.at[4 + q],
            )

    for copy in own_loads():
        copy.start()

    barrier = pltpu.get_barrier_semaphore()
    peers = [z_right, z_left, partner] + [{"tp": lax.rem(t + i, n_tp)} for i in range(1, n_tp)]
    for peer in peers:
        pl.semaphore_signal(barrier, inc=1, device_id=peer, device_id_type=MESH)
    pl.semaphore_wait(barrier, len(peers))

    for copy in own_loads():
        copy.wait()

    def piece(kind, f, share):
        r0 = pl.multiple_of(f * k_rows, k_rows)
        if kind == 0:
            cols = pl.ds(pl.multiple_of(parity * GU_X, LANES), GU_X) if share == 0 else pl.ds(2 * GU_X, gu.shape[1] - 2 * GU_X)
            return gu.at[pl.ds(r0, k_rows), cols]
        if kind == 1:
            rws = pl.ds(pl.multiple_of(parity * WD_X, 16), WD_X) if share == 0 else pl.ds(2 * WD_X, wd.shape[1] - 2 * WD_X)
            return wd.at[f // 2, rws, pl.ds(pl.multiple_of(lax.rem(f, 2) * LANES, LANES), LANES)]
        cols = pl.ds(pl.multiple_of(parity * VM_X, LANES), VM_X) if share == 0 else pl.ds(2 * VM_X, vm.shape[1] - 2 * VM_X)
        return vm.at[pl.ds(r0, k_rows), cols]

    def many(kind, share, count):
        if kind == 0:
            w = GU_X if share == 0 else gu.shape[1] - 2 * GU_X
            return gu.at[pl.ds(0, count * k_rows), pl.ds(0, w)]
        if kind == 1:
            r = WD_X if share == 0 else wd.shape[1] - 2 * WD_X
            return wd.at[pl.ds(0, count), pl.ds(0, r), pl.ds(0, LANES)]
        w = VM_X if share == 0 else vm.shape[1] - 2 * VM_X
        return vm.at[pl.ds(0, count * k_rows), pl.ds(0, w)]

    def origin(way, s):
        return lax.rem(z + n_fs - s, n_fs) if way == 0 else lax.rem(z + s, n_fs)

    def reach(way, share):
        return steps if way == share else steps - 1

    def z_copy(kind, way, share, s_next):
        ref = piece(kind, origin(way, s_next - 1), share)
        return remote(
            ref,
            ref,
            z_send.at[kind, way, share],
            z_recv.at[kind, way, share, s_next - 1],
            z_right if way == 0 else z_left,
        )

    def z_arrival(kind, way, share, s):
        ref = piece(kind, origin(way, s), share)
        return remote(
            ref, ref, z_send.at[kind, way, share], z_recv.at[kind, way, share, s - 1], z_right if way == 0 else z_left
        )

    def y_copy(kind, way, s):
        ref = piece(kind, origin(way, s), 0)
        return remote(ref, ref, y_send.at[kind, way], y_recv.at[kind, way], partner)

    def spread_mix(f):
        dest, b = f // 2, lax.rem(f, 2)
        src = vm.at[pl.ds(pl.multiple_of(f * k_rows, k_rows), k_rows), pl.ds(2 * chan_w, chan_w)]
        dst = mxb.at[
            pl.ds(pl.multiple_of(t * chan_w, chan_w), chan_w), pl.ds(pl.multiple_of(b * LANES, LANES), LANES)
        ]

        @pl.when(dest != t)
        def _():
            remote(src, dst, mx_send.at[0], mx_recv.at[t, b], {"tp": dest}).start()

        @pl.when(dest == t)
        def _():
            pltpu.make_async_copy(src, dst, mx_recv.at[t, b]).start()

    def relay(kinds, s, last):
        for share in range(2):
            for way in range(2):
                for kind in kinds:
                    far = reach(way, share)
                    if isinstance(s, int) and s > far:
                        continue
                    z_arrival(kind, way, share, s).wait_recv()
                    if not isinstance(s, int) or s < far:
                        z_copy(kind, way, share, s + 1).start()
                    if share == 0:
                        y_copy(kind, way, s).start()
                    if kind == 2 and share == 1:
                        spread_mix(origin(way, s))

    def relay_loop(kinds, lo, hi, extra=None):
        @pl.loop(lo, hi)
        def _(s):
            relay(kinds, s, None)
            if extra is not None:
                extra(s)

    def y_wait(kind):
        for way in range(2):
            ref = many(kind, 0, reach(way, 0))
            remote(ref, ref, y_send.at[kind, way], y_recv.at[kind, way], partner).wait_recv()

    def block(buf, w, q, b, part=None):
        rws = slice(None) if part is None else pl.ds(part * half, half)
        return buf.at[q, rws, pl.ds(pl.multiple_of(b * w, w), w)]

    def ag_copy(n, ref, q, s_i, r_i, where):
        return remote(ref, ref, ag_send.at[n, q, s_i], ag_recv.at[n, q, r_i], where)

    def ag_start(n, buf, w, q):
        own = block(buf, w, q, t)
        ag_copy(n, own, q, 1, 1, x_right).start()
        ag_copy(n, own, q, 2, 2, x_left).start()
        ag_copy(n, own, q, 0, 0, sib).start()

    def ag_relay(n, buf, w, q):
        b_l, b_r = 2 * xl + core, 2 * xr + core
        ag_copy(n, block(buf, w, q, b_l), q, 1, 1, x_right).wait_recv()
        ag_copy(n, block(buf, w, q, b_l, 0), q, 4, 3, x_right).start()
        ag_copy(n, block(buf, w, q, b_l), q, 3, 5, sib).start()
        ag_copy(n, block(buf, w, q, b_r), q, 2, 2, x_left).wait_recv()
        ag_copy(n, block(buf, w, q, b_r, 1), q, 6, 4, x_left).start()
        ag_copy(n, block(buf, w, q, b_r), q, 5, 6, sib).start()

    def ag_opposite(n, buf, w, q):
        b_o = 2 * xo + core
        ag_copy(n, block(buf, w, q, b_o, 0), q, 4, 3, x_right).wait_recv()
        ag_copy(n, block(buf, w, q, b_o, 0), q, 7, 7, sib).start()
        ag_copy(n, block(buf, w, q, b_o, 1), q, 6, 4, x_left).wait_recv()
        ag_copy(n, block(buf, w, q, b_o, 1), q, 8, 8, sib).start()

    def ag_end(n, buf, w, q):
        ag_copy(n, block(buf, w, q, 2 * x + other), q, 0, 0, sib).wait_recv()
        ag_copy(n, block(buf, w, q, 2 * xl + other), q, 3, 5, sib).wait_recv()
        ag_copy(n, block(buf, w, q, 2 * xr + other), q, 5, 6, sib).wait_recv()
        ag_copy(n, block(buf, w, q, 2 * xo + other, 0), q, 7, 7, sib).wait_recv()
        ag_copy(n, block(buf, w, q, 2 * xo + other, 1), q, 8, 8, sib).wait_recv()

    def ag_drain(n, buf, w, q):
        whole, part = block(buf, w, q, t), block(buf, w, q, t, 0)
        for i in range(9):
            ref = part if i in (4, 6, 7, 8) else whole
            ag_copy(n, ref, q, i, 0, sib).wait_send()

    def rs_copy(src, dst, n, q, i, where):
        return remote(src, dst, rs_send.at[n, q, i], rs_recv.at[n, q, i], where)

    order = (xo, xr, xl, x)
    sib_copy = lambda n, q, k: rs_copy(sdo.at[n, q, k], sdi.at[n, q, k], n, q, k, sib)

    def opp_copy(n, q, i):
        ref = pl.ds(i * half, half)
        return rs_copy(obo.at[n, q, ref], obi.at[n, q, ref], n, q, 4 + i, x_right if i == 0 else x_left)

    def nb_copy(n, q, i):
        return rs_copy(nbo.at[n, q, i], nbi.at[n, q, i], n, q, 6 + i, x_right if i == 0 else x_left)

    def rs_partials(n, q, base):
        h = hid[pl.ds(pl.multiple_of(base, 16), rows), :]
        for k in range(4):
            sdo[n, q, k] = jnp.dot(h, wd[2 * order[k] + other], preferred_element_type=F32).astype(BF16)
            sib_copy(n, q, k).start()
            acc[q, k] = jnp.dot(h, wd[2 * order[k] + core], preferred_element_type=F32)

    def rs_opposite(n, q):
        sib_copy(n, q, 0).wait_recv()
        obo[n, q] = (acc[q, 0] + sdi[n, q, 0].astype(F32)).astype(BF16)
        opp_copy(n, q, 0).start()
        opp_copy(n, q, 1).start()

    def rs_neighbours(n, q):
        for i in range(2):
            sib_copy(n, q, 1 + i).wait_recv()
            opp_copy(n, q, i).wait_recv()
            mine, far = pl.ds(i * half, half), pl.ds((1 - i) * half, half)
            nbo[n, q, i, mine] = (
                acc[q, 1 + i, mine] + sdi[n, q, 1 + i, mine].astype(F32) + obi[n, q, mine].astype(F32)
            ).astype(BF16)
            nbo[n, q, i, far] = (acc[q, 1 + i, far] + sdi[n, q, 1 + i, far].astype(F32)).astype(BF16)
            nb_copy(n, q, i).start()

    def rs_total(n, q):
        sib_copy(n, q, 3).wait_recv()
        nb_copy(n, q, 0).wait_recv()
        nb_copy(n, q, 1).wait_recv()
        return (
            acc[q, 3] + sdi[n, q, 3].astype(F32) + nbi[n, q, 0].astype(F32) + nbi[n, q, 1].astype(F32)
        )

    def rs_drain(n, q):
        for k in range(4):
            sib_copy(n, q, k).wait_send()
        for i in range(2):
            opp_copy(n, q, i).wait_send()
            nb_copy(n, q, i).wait_send()

    def norm_rows(buf, q, r, base):
        @pl.loop(0, rows // 16)
        def _(i):
            rws = pl.ds(pl.multiple_of(i * 16, 16), 16)
            v = buf[q, rws, :].astype(F32)
            inverse = lax.rsqrt(jnp.sum(v * v, axis=1, keepdims=True) / feat + EPS)
            ub[pl.ds(pl.multiple_of(base + i * 16, 16), 16), :] = (v * inverse * gf[r : r + 1, :]).astype(BF16)

    n_full = gu.shape[1] // (2 * LANES)
    tail = gu.shape[1] - n_full * 2 * LANES

    def hidden_tile(n, lo, count):
        c0 = pl.multiple_of(n * 2 * LANES, LANES)
        r = jnp.dot(ub[pl.ds(lo, count), :], gu[:, pl.ds(c0, 2 * LANES)], preferred_element_type=F32)
        a, b = r[:, :LANES], r[:, LANES:]
        hid[pl.ds(lo, count), pl.ds(pl.multiple_of(n * LANES, LANES), LANES)] = (jax.nn.silu(a) * b).astype(BF16)

    def hidden_tail(lo, count):
        r = jnp.dot(ub[pl.ds(lo, count), :], gu[:, n_full * 2 * LANES :], preferred_element_type=F32)
        a = pltpu.roll(r, tail // 2, 1)
        hid[pl.ds(lo, count), n_full * LANES :] = (jax.nn.silu(r) * a)[:, : tail // 2].astype(BF16)

    def conv(q):
        b0 = pl.multiple_of(q * rows, 16)
        r = jnp.dot(ub[pl.ds(b0, rows), :], vm[:, : 2 * chan_w], preferred_element_type=F32)
        glued = r[:, :chan_w] * jax.nn.sigmoid(r[:, chan_w:])
        for i in range(rows // LEN):
            pad[i, 32:, :] = glued[i * LEN : (i + 1) * LEN]
        n_taps = taps_in.shape[0]
        taps = taps_in[...].astype(F32)
        for i in range(rows // LEN):
            total = jnp.zeros((LEN, chan_w), F32)
            for k in range(n_taps):
                total = total + taps[k : k + 1, :] * pad[i, 33 - n_taps + k : 33 - n_taps + k + LEN, :]
            cvb[q, i * LEN : (i + 1) * LEN, pl.ds(pl.multiple_of(t * chan_w, chan_w), chan_w)] = total.astype(BF16)

    def channel_norm(q):
        @pl.loop(0, rows // 16)
        def _(i):
            rws = pl.ds(pl.multiple_of(i * 16, 16), 16)
            v = cvb[q, rws, :].astype(F32)
            mu = jnp.sum(v, axis=1, keepdims=True) / chan
            msq = jnp.sum(v * v, axis=1, keepdims=True) / chan
            w = (v - mu) * lax.rsqrt(msq - mu * mu + EPS) * cgb[3:4, :] + cgb[11:12, :]
            mixed[rws, :] = jax.nn.silu(w).astype(BF16)

    def own_cols(buf, q):
        return buf[q, :, pl.ds(pl.multiple_of(t * width, width), width)]

    def each(fn):
        pl.loop(0, nq)(fn)

    def z_begin(kinds):
        for kind in kinds:
            for share in range(2):
                for way in range(2):
                    z_copy(kind, way, share, 1).start()

    z_begin((0,))
    each(lambda q: ag_start(0, sb0, width, q))

    def pk_copy(i):
        return remote(pk.at[t], pk.at[t], pk_send.at[i - 1], pk_recv.at[t], {"tp": lax.rem(t + i, n_tp)})

    for i in range(1, n_tp):
        pk_copy(i).start()
    z_begin((1, 2))
    spread_mix(z)

    pad[:, :32, :] = jnp.zeros((pad.shape[0], 32, chan_w), F32)

    relay((0,), 1, None)
    each(lambda q: ag_relay(0, sb0, width, q))
    relay((0,), 2, None)
    each(lambda q: ag_opposite(0, sb0, width, q))
    for i in range(1, n_tp):
        b = lax.rem(t + i, n_tp)
        remote(pk.at[b], pk.at[b], pk_send.at[i - 1], pk_recv.at[b], {"tp": b}).wait_recv()
    for b in range(n_tp):
        gf[:, b * width : (b + 1) * width] = pk[b]
        cgb[0:8, b * chan_w : (b + 1) * chan_w] = pk[b][:, :chan_w]
        cgb[8:16, b * chan_w : (b + 1) * chan_w] = pk[b][:, chan_w : 2 * chan_w]
    relay((0,), 3, None)
    each(lambda q: ag_end(0, sb0, width, q))

    def early_norm(s):
        q = s - 4

        @pl.when(q < nq)
        def _():
            norm_rows(sb0, q, 0, q * rows)

    relay_loop((0,), 4, steps - 1, early_norm)
    for s in (steps - 1, steps):
        relay((0,), s, None)

    relay_loop((1, 2), 1, 4)
    y_wait(0)

    tokens = nq * rows

    def tiles(s):
        hidden_tile(2 * (s - 4), 0, tokens)

        @pl.when(2 * (s - 4) + 1 < n_full)
        def _():
            hidden_tile(2 * (s - 4) + 1, 0, tokens)

    relay_loop((1, 2), 4, steps - 1, tiles)
    hidden_tail(0, tokens)
    for s in (steps - 1, steps):
        relay((1, 2), s, None)
    y_wait(1)

    each(lambda q: rs_partials(0, q, q * rows))
    each(lambda q: rs_opposite(0, q))
    each(lambda q: rs_neighbours(0, q))

    def first(q):
        total = rs_total(0, q)
        sb1[q, :, pl.ds(pl.multiple_of(t * width, width), width)] = (
            own_cols(sb0, q).astype(F32) + 0.5 * total
        ).astype(BF16)
        ag_start(1, sb1, width, q)

    each(first)
    each(lambda q: ag_relay(1, sb1, width, q))
    y_wait(2)
    each(lambda q: ag_opposite(1, sb1, width, q))

    def conv_stage(q):
        ag_end(1, sb1, width, q)
        norm_rows(sb1, q, 1, q * rows)
        conv(q)
        ag_start(2, cvb, chan_w, q)

    each(conv_stage)
    each(lambda q: ag_relay(2, cvb, chan_w, q))
    each(lambda q: ag_opposite(2, cvb, chan_w, q))

    for b in range(n_tp):
        for i in range(2):
            ref = mxb.at[pl.ds(b * chan_w, chan_w), pl.ds(i * LANES, LANES)]
            pltpu.make_async_copy(ref, ref, mx_recv.at[b, i]).wait()

    def mix_stage(q):
        ag_end(2, cvb, chan_w, q)
        channel_norm(q)
        branch = jnp.dot(mixed[...], mxb[...], preferred_element_type=F32)
        sb3[q, :, pl.ds(pl.multiple_of(t * width, width), width)] = (
            own_cols(sb1, q).astype(F32) + branch
        ).astype(BF16)
        ag_start(3, sb3, width, q)

    each(mix_stage)
    each(lambda q: ag_relay(3, sb3, width, q))
    each(lambda q: ag_opposite(3, sb3, width, q))

    def ffn_stage(q):
        base = pl.multiple_of(q * rows, 16)
        ag_end(3, sb3, width, q)
        norm_rows(sb3, q, 2, base)

        @pl.loop(0, n_full)
        def _(n):
            hidden_tile(n, base, rows)

        hidden_tail(base, rows)
        rs_partials(1, q, base)

    each(ffn_stage)
    each(lambda q: rs_opposite(1, q))
    each(lambda q: rs_neighbours(1, q))

    def last(q):
        total = rs_total(1, q)
        out[pl.ds(pl.multiple_of(q * rows, 16), rows), :] = (
            own_cols(sb3, q).astype(F32) + 0.5 * total
        ).astype(BF16)

    each(last)

    for kind in range(3):
        for way in range(2):
            for share in range(2):
                ref = many(kind, share, reach(way, share))
                remote(ref, ref, z_send.at[kind, way, share], z_recv.at[kind, way, share, 0], z_right).wait_send()
            ref = many(kind, 0, reach(way, 0))
            remote(ref, ref, y_send.at[kind, way], y_recv.at[kind, way], partner).wait_send()
    for i in range(1, n_tp):
        pk_copy(i).wait_send()
    ref = mxb.at[pl.ds(0, (n_tp - 1) * chan_w), :]
    remote(ref, ref, mx_send.at[0], mx_recv.at[0, 0], sib).wait_send()

    def drain(q):
        for n, buf, w in ((0, sb0, width), (1, sb1, width), (2, cvb, chan_w), (3, sb3, width)):
            ag_drain(n, buf, w, q)
        for n in range(2):
            rs_drain(n, q)

    each(drain)


def solution(mesh):
    n_fs, n_tp = mesh.shape["fs"], mesh.shape["tp"]

    def local(
        stream_in,
        gain_before,
        gain_mixer,
        gain_after,
        w_gate,
        w_upward,
        w_down,
        w_value,
        w_glu_gate,
        conv_taps,
        chan_gain,
        chan_bias,
        w_mix_out,
    ):
        tokens, width = stream_in.shape
        k_rows, hidden = w_gate.shape
        chan_w = w_value.shape[1]
        pieces = []
        for c in range(0, hidden, LANES):
            pieces += [w_gate[:, c : c + LANES], w_upward[:, c : c + LANES]]
        gu_in = jnp.concatenate(pieces, axis=1)
        vm_in = jnp.concatenate([w_value, w_glu_gate, w_mix_out], axis=1)
        zero = jnp.zeros((4, width), F32)
        pk_in = jnp.concatenate(
            [
                gain_before[None].astype(F32),
                gain_mixer[None].astype(F32),
                gain_after[None].astype(F32),
                jnp.concatenate([chan_gain, chan_bias])[None].astype(F32),
                zero,
            ],
            axis=0,
        )
        nq = CHUNKS
        rows = tokens // nq
        feat, chan = width * n_tp, chan_w * n_tp
        vmem = pltpu.VMEM
        dma = pltpu.SemaphoreType.DMA
        any_space = pl.BlockSpec(memory_space=pl.ANY)
        in_vmem = pl.BlockSpec(memory_space=pltpu.VMEM)
        return pl.pallas_call(
            lambda *refs: layer_kernel(n_fs, n_tp, *refs),
            out_shape=jax.ShapeDtypeStruct((tokens, width), BF16),
            in_specs=[any_space] * 5 + [in_vmem],
            out_specs=in_vmem,
            scratch_shapes=[
                vmem((n_fs * k_rows, 2 * hidden), BF16),
                vmem((n_fs // 2, hidden, 2 * LANES), BF16),
                vmem((n_fs * k_rows, 3 * chan_w), BF16),
                vmem((chan, 2 * LANES), BF16),
                vmem((n_tp, 8, width), F32),
                vmem((8, feat), F32),
                vmem((16, chan), F32),
                vmem((nq, rows, feat), BF16),
                vmem((nq, rows, feat), BF16),
                vmem((nq, rows, feat), BF16),
                vmem((nq, rows, chan), BF16),
                vmem((tokens, feat), BF16),
                vmem((rows, chan), BF16),
                vmem((tokens, hidden), BF16),
                vmem((rows // LEN, LEN + 32, chan_w), F32),
                vmem((2, nq, 4, rows, width), BF16),
                vmem((2, nq, 4, rows, width), BF16),
                vmem((nq, 4, rows, width), F32),
                vmem((2, nq, rows, width), BF16),
                vmem((2, nq, rows, width), BF16),
                vmem((2, nq, 2, rows, width), BF16),
                vmem((2, nq, 2, rows, width), BF16),
                dma((4 + nq,)),
                dma((3, 2, 2, n_fs // 2)),
                dma((3, 2, 2)),
                dma((3, 2)),
                dma((3, 2)),
                dma((n_tp,)),
                dma((n_tp - 1,)),
                dma((n_tp, 2)),
                dma((1,)),
                dma((4, nq, 9)),
                dma((4, nq, 9)),
                dma((2, nq, 8)),
                dma((2, nq, 8)),
            ],
            compiler_params=pltpu.CompilerParams(
                collective_id=0, has_side_effects=True, vmem_limit_bytes=60 * 1024 * 1024
            ),
        )(stream_in, gu_in, w_down, vm_in, pk_in, conv_taps)

    in_specs = (
        P(("grp", "fs"), "tp"),
        P("tp"),
        P("tp"),
        P("tp"),
        P("fs", "tp"),
        P("fs", "tp"),
        P("tp", "fs"),
        P("fs", "tp"),
        P("fs", "tp"),
        P(None, "tp"),
        P("tp"),
        P("tp"),
        P("tp", "fs"),
    )
    out_specs = P(("grp", "fs"), "tp")
    return jax.shard_map(local, mesh=mesh, in_specs=in_specs, out_specs=out_specs, check_vma=False)
```

time: 408 us -> 186 us (0.46)
  Pallas kernels: 0 us -> 176 us
  waiting for transfers between devices: 165 us -> 0 us
  blocking collectives: 140 us -> 0 us
  starting transfers between devices: 52.1 us -> 0 us
  matrix products: 24 us -> 0 us
  between operations: 13.4 us -> 0.14 us
  other arithmetic: 7.32 us -> 0.67 us
    pallas_call x0 -> x1, Pallas kernels: none -> 176 us  [local(): pl.pallas_call(lambda *refs: layer_kernel(n_fs, n_tp, *refs), out_shape=j...]
    all_gather x3 -> x0, waiting for transfers between devices: 131 us -> none  [the longest x1 75 us: local(): whole_down = lax.all_gather(w_down, 'fs', axis=1, tiled=True)]
    all_to_all x4 -> x0, blocking collectives: 95.4 us -> none  [the longest x2 47.8 us: sent_and_summed(): lax.all_to_all(parts, axis, split_axis=0, concat_axis=0, tiled=True)]
    all_to_all x5 -> x0, starting transfers between devices: 52 us -> none  [the longest x4 36.5 us: from_everyone(): return lax.all_to_all(copies, axis, split_axis=0, concat_axis=0, tiled=True)]
    all_to_all x5 -> x0, waiting for transfers between devices: 33.3 us -> none  [the longest x1 19.8 us: sent_and_summed(): lax.all_to_all(parts, axis, split_axis=0, concat_axis=0, tiled=True)]
    all_gather x1 -> x0, blocking collectives: 26 us -> none  [local(): lax.all_gather(w_mix_out, 'fs', axis=1, tiled=True)]
    dot_general x7 -> x0, matrix products: 24 us -> none  [the longest x2 12.1 us: feed_forward(): jnp.dot(hidden, whole_down, preferred_element_type=jnp.float32)]
    psum x1 -> x0, blocking collectives: 18.3 us -> none  [local(): lax.psum((jnp.sum(flat, axis=1), jnp.sum(flat * flat, axis=1)), 'tp')]
  transfers between devices with their start and end apart: 8 -> 0, of which waited for: 6 -> 0; matrix products, arithmetic and copies ran while one was open for 3% -> 0% of each run, Pallas kernels for 0% -> 0%
where the time goes in v1:
time: 186 us; the launch traced here: 185 us
  Pallas kernels  176 us (95%)
  local copies, waits for them, and re-layouts  8.81 us (5%)
    pallas_call x1, Pallas kernels, local(): pl.pallas_call(lambda *refs: layer_kernel(n_fs, n_tp, *refs), out_shape=j...  176 us
    unnamed x31, local copies, waits for them, and re-layouts  5.04 us

profile of v1, /device:TPU:33, one launch (start us, length us, event | category | flops | bytes accessed | tf_op | source)
XLA Modules:
  0.0 185.5 jit_solution(16251290849387549705)
XLA Ops:
  0.0 0.9 fusion.1
  0.9 0.1 copy.26
  1.0 0.1 copy.27
  1.1 0.1 copy.28
  1.3 0.1 copy.29
  1.4 0.1 copy.30
  1.5 0.1 copy.31
  1.6 0.1 copy.32
  1.8 0.1 copy.33
  1.9 0.1 copy.34
  2.0 0.1 copy.35
  2.2 0.7 slice-done
  2.9 0.1 copy.36
  3.0 0.7 slice-done.1
  3.7 0.1 copy.37
  3.9 0.8 concatenate.23.refs_1_
  4.7 0.7 pad_maximum_fusion.refs_3_
  5.4 0.7 copy-done.7
  6.0 0.7 copy-done.8
  6.7 0.7 copy-done.4
  7.4 0.0 copy-done.5
  7.4 0.6 concatenate.28.refs_4_
  8.0 175.8 %shard_map.127 = bf16[384,256]{1,0:T(8,128)(2,1)} custom-call(bf16[384,256]{1,0:T(8,128)(2,1)} %refs_0_.1, bf16[128,1408]{1,0:T(8,128)(2,1)} %concatenate.23.refs_1_, bf16[704,128]{1,0:T(8,128)(2,1)} %refs_2_.1, bf16[128,384]{1,0:T(8,128)(2,1)} %pad_maximum_fusion.refs_3_, f32[8,256]{1,0:T(8,128)} %concatenate.28.refs_4_, bf16[31,128]{1,0:T(8,128)(2,1)} %refs_5_.1), custom_call_target="tpu_custom_call" | custom-call | tf_op jit(solution)/shard_map/pallas_call | solution.py:551
  183.8 1.6 copy.39
  (22 shorter events, 0.1 us)
Async XLA Ops:
  0.0 1.0 copy-start
  2.1 0.7 slice-start
  3.0 0.7 slice-start.1
  3.8 0.9 copy-start.1
  3.8 0.9 copy-start.2
  3.9 0.9 copy-start.3
  4.7 0.7 copy-start.6
  5.4 0.7 copy-start.7
  6.0 0.7 copy-start.8
  6.7 0.7 copy-start.4
  6.7 0.7 copy-start.5

commit v2 on v1

--- a/solution.py
+++ b/solution.py
@@ -30,11 +30,18 @@
     n_fs,
     n_tp,
     s_in,
-    gu_in,
+    gate_in,
+    up_in,
     wd_in,
-    vm_in,
-    pk_in,
+    value_in,
+    glu_in,
+    mix_in,
     taps_in,
+    before_in,
+    mixer_in,
+    after_in,
+    cgain_in,
+    cbias_in,
     out,
     gu,
     wd,
@@ -87,18 +94,18 @@
     nq, rows, width = sb0.shape[0], sb0.shape[1], s_in.shape[1]
     half = rows // 2
     feat = width * n_tp
-    k_rows = gu_in.shape[0]
-    chan_w = vm_in.shape[1] // 3
+    k_rows, chan_w = value_in.shape
     chan = chan_w * n_tp
     steps = n_fs // 2
 
+    own_k = pl.ds(pl.multiple_of(z * k_rows, k_rows), k_rows)
+
     def own_loads():
-        yield pltpu.make_async_copy(gu_in, gu.at[pl.ds(pl.multiple_of(z * k_rows, k_rows), k_rows), :], load_sem.at[0])
         yield pltpu.make_async_copy(
-            wd_in, wd.at[z // 2, :, pl.ds(pl.multiple_of(lax.rem(z, 2) * LANES, LANES), LANES)], load_sem.at[1]
+            wd_in, wd.at[z // 2, :, pl.ds(pl.multiple_of(lax.rem(z, 2) * LANES, LANES), LANES)], load_sem.at[0]
         )
-        yield pltpu.make_async_copy(vm_in, vm.at[pl.ds(pl.multiple_of(z * k_rows, k_rows), k_rows), :], load_sem.at[2])
-        yield pltpu.make_async_copy(pk_in, pk.at[t], load_sem.at[3])
+        for i, ref in enumerate((value_in, glu_in, mix_in)):
+            yield pltpu.make_async_copy(ref, vm.at[own_k, i * chan_w : (i + 1) * chan_w], load_sem.at[1 + i])
         for q in range(nq):
             yield pltpu.make_async_copy(
                 s_in.at[pl.ds(q * rows, rows), :],
@@ -108,6 +115,21 @@
 
     for copy in own_loads():
         copy.start()
+
+    hidden = gate_in.shape[0]
+    n_full = hidden // LANES
+    for n in range(n_full):
+        r = slice(n * LANES, (n + 1) * LANES)
+        gu[own_k, 2 * n * LANES : (2 * n + 1) * LANES] = gate_in[r, :].T
+        gu[own_k, (2 * n + 1) * LANES : (2 * n + 2) * LANES] = up_in[r, :].T
+    gu[own_k, 2 * n_full * LANES :] = jnp.concatenate(
+        [gate_in[n_full * LANES :, :], up_in[n_full * LANES :, :]], axis=0
+    ).T
+    for i, ref in enumerate((before_in, mixer_in, after_in)):
+        pk[t, i : i + 1, :] = ref[...].astype(F32).reshape(1, width)
+    pk[t, 3:4, :chan_w] = cgain_in[...].astype(F32).reshape(1, chan_w)
+    pk[t, 3:4, chan_w:] = cbias_in[...].astype(F32).reshape(1, chan_w)
+    pk[t, 4:8, :] = jnp.zeros((4, width), F32)
 
     barrier = pltpu.get_barrier_semaphore()
     peers = [z_right, z_left, partner] + [{"tp": lax.rem(t + i, n_tp)} for i in range(1, n_tp)]
@@ -302,26 +324,24 @@
             nb_copy(n, q, i).wait_send()
 
     def norm_rows(buf, q, r, base):
-        @pl.loop(0, rows // 16)
+        @pl.loop(0, rows // 16, unroll=4)
         def _(i):
             rws = pl.ds(pl.multiple_of(i * 16, 16), 16)
             v = buf[q, rws, :].astype(F32)
             inverse = lax.rsqrt(jnp.sum(v * v, axis=1, keepdims=True) / feat + EPS)
             ub[pl.ds(pl.multiple_of(base + i * 16, 16), 16), :] = (v * inverse * gf[r : r + 1, :]).astype(BF16)
 
-    n_full = gu.shape[1] // (2 * LANES)
-    tail = gu.shape[1] - n_full * 2 * LANES
-
-    def hidden_tile(n, lo, count):
-        c0 = pl.multiple_of(n * 2 * LANES, LANES)
-        r = jnp.dot(ub[pl.ds(lo, count), :], gu[:, pl.ds(c0, 2 * LANES)], preferred_element_type=F32)
-        a, b = r[:, :LANES], r[:, LANES:]
-        hid[pl.ds(lo, count), pl.ds(pl.multiple_of(n * LANES, LANES), LANES)] = (jax.nn.silu(a) * b).astype(BF16)
-
-    def hidden_tail(lo, count):
-        r = jnp.dot(ub[pl.ds(lo, count), :], gu[:, n_full * 2 * LANES :], preferred_element_type=F32)
-        a = pltpu.roll(r, tail // 2, 1)
-        hid[pl.ds(lo, count), n_full * LANES :] = (jax.nn.silu(r) * a)[:, : tail // 2].astype(BF16)
+    def hidden_part(lo, count, first, tiles, tail):
+        c0 = first * 2 * LANES
+        c1 = gu.shape[1] if tail else (first + tiles) * 2 * LANES
+        r = jnp.dot(ub[pl.ds(lo, count), :], gu[:, c0:c1], preferred_element_type=F32)
+        for n in range(tiles):
+            a, b = r[:, 2 * n * LANES : (2 * n + 1) * LANES], r[:, (2 * n + 1) * LANES : (2 * n + 2) * LANES]
+            hid[pl.ds(lo, count), (first + n) * LANES : (first + n + 1) * LANES] = (jax.nn.silu(a) * b).astype(BF16)
+        if tail:
+            r = r[:, 2 * tiles * LANES :]
+            w = r.shape[1]
+            hid[pl.ds(lo, count), n_full * LANES :] = (jax.nn.silu(r) * pltpu.roll(r, w // 2, 1))[:, : w // 2].astype(BF16)
 
     def conv(q):
         b0 = pl.multiple_of(q * rows, 16)
@@ -338,7 +358,7 @@
             cvb[q, i * LEN : (i + 1) * LEN, pl.ds(pl.multiple_of(t * chan_w, chan_w), chan_w)] = total.astype(BF16)
 
     def channel_norm(q):
-        @pl.loop(0, rows // 16)
+        @pl.loop(0, rows // 16, unroll=4)
         def _(i):
             rws = pl.ds(pl.multiple_of(i * 16, 16), 16)
             v = cvb[q, rws, :].astype(F32)
@@ -402,15 +422,9 @@
 
     tokens = nq * rows
 
-    def tiles(s):
-        hidden_tile(2 * (s - 4), 0, tokens)
-
-        @pl.when(2 * (s - 4) + 1 < n_full)
-        def _():
-            hidden_tile(2 * (s - 4) + 1, 0, tokens)
-
-    relay_loop((1, 2), 4, steps - 1, tiles)
-    hidden_tail(0, tokens)
+    for s, (a, b, tail) in zip((4, 5, 6), ((0, 2, False), (2, 2, False), (4, n_full - 4, True))):
+        relay((1, 2), s, None)
+        hidden_part(0, tokens, a, b, tail)
     for s in (steps - 1, steps):
         relay((1, 2), s, None)
     y_wait(1)
@@ -464,11 +478,7 @@
         ag_end(3, sb3, width, q)
         norm_rows(sb3, q, 2, base)
 
-        @pl.loop(0, n_full)
-        def _(n):
-            hidden_tile(n, base, rows)
-
-        hidden_tail(base, rows)
+        hidden_part(base, rows, 0, n_full, True)
         rs_partials(1, q, base)
 
     each(ffn_stage)
@@ -525,22 +535,6 @@
         tokens, width = stream_in.shape
         k_rows, hidden = w_gate.shape
         chan_w = w_value.shape[1]
-        pieces = []
-        for c in range(0, hidden, LANES):
-            pieces += [w_gate[:, c : c + LANES], w_upward[:, c : c + LANES]]
-        gu_in = jnp.concatenate(pieces, axis=1)
-        vm_in = jnp.concatenate([w_value, w_glu_gate, w_mix_out], axis=1)
-        zero = jnp.zeros((4, width), F32)
-        pk_in = jnp.concatenate(
-            [
-                gain_before[None].astype(F32),
-                gain_mixer[None].astype(F32),
-                gain_after[None].astype(F32),
-                jnp.concatenate([chan_gain, chan_bias])[None].astype(F32),
-                zero,
-            ],
-            axis=0,
-        )
         nq = CHUNKS
         rows = tokens // nq
         feat, chan = width * n_tp, chan_w * n_tp
@@ -551,7 +545,7 @@
         return pl.pallas_call(
             lambda *refs: layer_kernel(n_fs, n_tp, *refs),
             out_shape=jax.ShapeDtypeStruct((tokens, width), BF16),
-            in_specs=[any_space] * 5 + [in_vmem],
+            in_specs=[any_space, in_vmem, in_vmem] + [any_space] * 4 + [in_vmem] * 6,
             out_specs=in_vmem,
             scratch_shapes=[
                 vmem((n_fs * k_rows, 2 * hidden), BF16),
@@ -593,7 +587,21 @@
             compiler_params=pltpu.CompilerParams(
                 collective_id=0, has_side_effects=True, vmem_limit_bytes=60 * 1024 * 1024
             ),
-        )(stream_in, gu_in, w_down, vm_in, pk_in, conv_taps)
+        )(
+            stream_in,
+            w_gate.T,
+            w_upward.T,
+            w_down,
+            w_value,
+            w_glu_gate,
+            w_mix_out,
+            conv_taps,
+            gain_before,
+            gain_mixer,
+            gain_after,
+            chan_gain,
+            chan_bias,
+        )
 
     in_specs = (
         P(("grp", "fs"), "tp"),

time: 186 us -> 172 us (0.925)
  local copies, waits for them, and re-layouts: 8.81 us -> 1.62 us
  Pallas kernels: 176 us -> 170 us
    pallas_call x1, Pallas kernels: 176 us -> 170 us  [local(): pl.pallas_call(lambda *refs: layer_kernel(n_fs, n_tp, *refs), out_shape=j...]
    unnamed x31 -> x1, local copies, waits for them, and re-layouts: 5.04 us -> 1.62 us
    slice x6 -> x0, local copies, waits for them, and re-layouts: 2.33 us -> none  [local(): pieces += [w_gate[:, c:c + LANES], w_upward[:, c:c + LANES]]]
where the time goes in v2:
time: 172 us; the launch traced here: 171 us
  Pallas kernels  170 us (99%)
    pallas_call x1, Pallas kernels, local(): pl.pallas_call(lambda *refs: layer_kernel(n_fs, n_tp, *refs), out_shape=j...  170 us

profile of v2, /device:TPU:33, one launch (start us, length us, event | category | flops | bytes accessed | tf_op | source)
XLA Modules:
  0.0 171.4 jit_solution(3259154451963244770)
XLA Ops:
  0.0 169.8 %shard_map.127 = bf16[384,256]{1,0:T(8,128)(2,1)} custom-call(bf16[384,256]{1,0:T(8,128)(2,1)} %refs_0_.1, bf16[704,128]{1,0:T(8,128)(2,1)} %bitcast.2, bf16[704,128]{1,0:T(8,128)(2,1)} %bitcast.3, bf16[704,128]{1,0:T(8,128)(2,1)} %refs_3_.1, bf16[128,128]{1,0:T(8,128)(2,1)} %refs_4_.1, bf16[128,128]{1,0:T(8,128)(2,1)} %refs_5_.1, bf16[128,128]{1,0:T(8,128)(2,1)} %refs_6_.1, ...), custom_call_target="tpu_custom_call" | custom-call | tf_op jit(solution)/shard_map/pallas_call | solution.py:545
  169.8 1.6 copy.15

commit v3 on v2

v3 whole, which is shorter than its diff:
```python
import jax
import jax.numpy as jnp
from jax import lax
from jax.experimental import pallas as pl
from jax.experimental.pallas import tpu as pltpu
from jax.sharding import PartitionSpec as P

MESH = pl.DeviceIdType.MESH
LEN = 128
EPS = 1e-06
LANES = 128
CHUNKS = 3
BF16, F32 = jnp.bfloat16, jnp.float32


def remote(src, dst, send_sem, recv_sem, where):
    return pltpu.make_async_remote_copy(
        src_ref=src,
        dst_ref=dst,
        send_sem=send_sem,
        recv_sem=recv_sem,
        device_id=where,
        device_id_type=MESH,
    )


def layer_kernel(
    n_fs,
    n_tp,
    s_in,
    gate_in,
    up_in,
    wd_in,
    value_in,
    glu_in,
    mix_in,
    taps_in,
    before_in,
    mixer_in,
    after_in,
    cgain_in,
    cbias_in,
    out,
    gu,
    wd,
    vm,
    mxb,
    pk,
    gf,
    cgb,
    sb0,
    sb1,
    sb3,
    cvb,
    ub,
    mixed,
    hid,
    pad,
    ybo,
    ybi,
    acc,
    rs0,
    rs1,
    load_sem,
    z_recv,
    z_send,
    y_recv,
    y_send,
    pk_recv,
    pk_send,
    mx_recv,
    mx_send,
    ag_recv,
    ag_send,
    rs_recv,
    rs_send,
    yx_recv,
    yx_send,
):
    z, t, g = lax.axis_index("fs"), lax.axis_index("tp"), lax.axis_index("grp")
    parity = lax.rem(g, 2)
    partner = {"grp": g + 1 - 2 * parity}
    z_right = {"fs": lax.rem(z + 1, n_fs)}
    z_left = {"fs": lax.rem(z + n_fs - 1, n_fs)}
    chips = n_tp // 2
    x, core = t // 2, lax.rem(t, 2)
    xr, xl, xo = lax.rem(x + 1, chips), lax.rem(x + 3, chips), lax.rem(x + 2, chips)
    other = 1 - core
    sib = {"tp": 2 * x + other}
    x_right, x_left = {"tp": 2 * xr + core}, {"tp": 2 * xl + core}

    nq, rows, width = sb1.shape[0], sb1.shape[1], s_in.shape[1]
    half = rows // 2
    feat = width * n_tp
    k_rows, chan_w = value_in.shape
    chan = chan_w * n_tp
    steps = n_fs // 2
    own_units = gate_in.shape[0] // 2
    units = wd.shape[1] // 2
    pairs = units // LANES
    mine, theirs = parity, 1 - parity

    own_k = pl.ds(pl.multiple_of(z * k_rows, k_rows), k_rows)

    own_w = pl.ds(pl.multiple_of(t * width, width), width)

    def own_loads():
        for h in range(2):
            yield pltpu.make_async_copy(
                wd_in.at[h * own_units : (h + 1) * own_units, :],
                wd.at[
                    z // 2,
                    h * units : h * units + own_units,
                    pl.ds(pl.multiple_of(lax.rem(z, 2) * LANES, LANES), LANES),
                ],
                load_sem.at[h],
            )
        for i, ref in enumerate((value_in, glu_in, mix_in)):
            yield pltpu.make_async_copy(ref, vm.at[own_k, i * chan_w : (i + 1) * chan_w], load_sem.at[2 + i])
        for q in range(nq):
            yield pltpu.make_async_copy(
                s_in.at[pl.ds(q * rows, rows), :],
                sb0.at[nq + q, :, pl.ds(pl.multiple_of(t * width, width), width)],
                load_sem.at[5 + q],
            )

    for copy in own_loads():
        copy.start()

    for h in range(2):
        for i in range(pairs):
            lo = h * own_units + i * LANES
            hi = min(lo + LANES, (h + 1) * own_units)
            for j, ref in enumerate((gate_in, up_in)):
                v = ref[lo:hi, :]
                if hi - lo < LANES:
                    v = jnp.concatenate([v, jnp.zeros((LANES - hi + lo, k_rows), BF16)], axis=0)
                c = h * 2 * units + (2 * i + j) * LANES
                gu[own_k, c : c + LANES] = v.T
        wd[:, h * units + own_units : (h + 1) * units, :] = jnp.zeros((wd.shape[0], units - own_units, wd.shape[2]), BF16)
    for i, ref in enumerate((before_in, mixer_in, after_in)):
        pk[t, i : i + 1, :] = ref[...].astype(F32).reshape(1, width)
    pk[t, 3:4, :chan_w] = cgain_in[...].astype(F32).reshape(1, chan_w)
    pk[t, 3:4, chan_w:] = cbias_in[...].astype(F32).reshape(1, chan_w)
    pk[t, 4:8, :] = jnp.zeros((4, width), F32)

    barrier = pltpu.get_barrier_semaphore()
    peers = [z_right, z_left, partner] + [{"tp": lax.rem(t + i, n_tp)} for i in range(1, n_tp)]
    for peer in peers:
        pl.semaphore_signal(barrier, inc=1, device_id=peer, device_id_type=MESH)
    pl.semaphore_wait(barrier, len(peers))

    for copy in own_loads():
        copy.wait()

    wide = 2 * LANES * (pairs - 1)
    third = own_units // 2

    def piece(kind, f, share):
        r0 = pl.ds(pl.multiple_of(f * k_rows, k_rows), k_rows)
        if kind == 0:
            c0 = mine * 2 * units
            if share == 0:
                return gu.at[r0, pl.ds(pl.multiple_of(c0, LANES), wide)]
            return gu.at[r0, pl.ds(pl.multiple_of(c0 + wide, LANES), 2 * units - wide)]
        if kind == 2:
            return vm.at[r0, 0 : 2 * chan_w] if share == 0 else vm.at[r0, 2 * chan_w : 3 * chan_w]
        q0 = (mine if kind == 1 else theirs) * units + share * third
        return wd.at[
            f // 2,
            pl.ds(pl.multiple_of(q0, 16), third),
            pl.ds(pl.multiple_of(lax.rem(f, 2) * LANES, LANES), LANES),
        ]

    def many(kind, share, count):
        if kind == 0:
            return gu.at[0 : count * k_rows, 0 : (wide if share == 0 else 2 * units - wide)]
        if kind == 2:
            return vm.at[0 : count * k_rows, 0 : (2 * chan_w if share == 0 else chan_w)]
        return wd.at[0:count, 0:third, 0:LANES]

    def origin(way, s):
        return lax.rem(z + n_fs - s, n_fs) if way == 0 else lax.rem(z + s, n_fs)

    def reach(way, share):
        return steps if way == share else steps - 1

    def z_copy(kind, way, share, s_next):
        ref = piece(kind, origin(way, s_next - 1), share)
        return remote(
            ref,
            ref,
            z_send.at[kind, way, share],
            z_recv.at[kind, way, share, s_next - 1],
            z_right if way == 0 else z_left,
        )

    def z_arrival(kind, way, share, s):
        ref = piece(kind, origin(way, s), share)
        return remote(
            ref, ref, z_send.at[kind, way, share], z_recv.at[kind, way, share, s - 1], z_right if way == 0 else z_left
        )

    def y_copy(way, s):
        ref = piece(0, origin(way, s), 0)
        return remote(ref, ref, y_send.at[way], y_recv.at[way], partner)

    def y_late(f):
        ref = piece(0, f, 1)
        return remote(ref, ref, y_send.at[2], y_recv.at[2], partner)

    def y_all(i):
        ref = many(0, 0, reach(i, 0)) if i < 2 else many(0, 1, n_fs - 1)
        return remote(ref, ref, y_send.at[i], y_recv.at[i], partner)

    def stream_copy(q):
        return remote(
            sb0.at[nq + q, :, own_w], sb0.at[q, :, own_w], yx_send.at[0, q], yx_recv.at[0, q], partner
        )

    def part_copy(q):
        return remote(ybo.at[q], ybi.at[q], yx_send.at[1, q], yx_recv.at[1, q], partner)

    def spread_mix(f):
        dest, b = f // 2, lax.rem(f, 2)
        src = vm.at[pl.ds(pl.multiple_of(f * k_rows, k_rows), k_rows), pl.ds(2 * chan_w, chan_w)]
        dst = mxb.at[
            pl.ds(pl.multiple_of(t * chan_w, chan_w), chan_w), pl.ds(pl.multiple_of(b * LANES, LANES), LANES)
        ]

        @pl.when(dest != t)
        def _():
            remote(src, dst, mx_send.at[0], mx_recv.at[t, b], {"tp": dest}).start()

        @pl.when(dest == t)
        def _():
            pltpu.make_async_copy(src, dst, mx_recv.at[t, b]).start()

    def relay(kinds, s, last):
        for share in range(2):
            for way in range(2):
                for kind in kinds:
                    far = reach(way, share)
                    if isinstance(s, int) and s > far:
                        continue
                    z_arrival(kind, way, share, s).wait_recv()
                    if not isinstance(s, int) or s < far:
                        z_copy(kind, way, share, s + 1).start()
                    if kind == 0 and share == 0:
                        y_copy(way, s).start()
                    if kind == 2 and share == 1:
                        spread_mix(origin(way, s))

    def block(buf, w, q, b, part=None):
        rws = slice(None) if part is None else pl.ds(part * half, half)
        return buf.at[q, rws, pl.ds(pl.multiple_of(b * w, w), w)]

    def ag_copy(n, ref, q, s_i, r_i, where):
        return remote(ref, ref, ag_send.at[n, q, s_i], ag_recv.at[n, q, r_i], where)

    def ag_start(n, buf, w, q):
        own = block(buf, w, q, t)
        ag_copy(n, own, q, 1, 1, x_right).start()
        ag_copy(n, own, q, 2, 2, x_left).start()
        ag_copy(n, own, q, 0, 0, sib).start()

    def ag_relay(n, buf, w, q):
        b_l, b_r = 2 * xl + core, 2 * xr + core
        ag_copy(n, block(buf, w, q, b_l), q, 1, 1, x_right).wait_recv()
        ag_copy(n, block(buf, w, q, b_l, 0), q, 4, 3, x_right).start()
        ag_copy(n, block(buf, w, q, b_l), q, 3, 5, sib).start()
        ag_copy(n, block(buf, w, q, b_r), q, 2, 2, x_left).wait_recv()
        ag_copy(n, block(buf, w, q, b_r, 1), q, 6, 4, x_left).start()
        ag_copy(n, block(buf, w, q, b_r), q, 5, 6, sib).start()

    def ag_opposite(n, buf, w, q):
        b_o = 2 * xo + core
        ag_copy(n, block(buf, w, q, b_o, 0), q, 4, 3, x_right).wait_recv()
        ag_copy(n, block(buf, w, q, b_o, 0), q, 7, 7, sib).start()
        ag_copy(n, block(buf, w, q, b_o, 1), q, 6, 4, x_left).wait_recv()
        ag_copy(n, block(buf, w, q, b_o, 1), q, 8, 8, sib).start()

    def ag_end(n, buf, w, q):
        ag_copy(n, block(buf, w, q, 2 * x + other), q, 0, 0, sib).wait_recv()
        ag_copy(n, block(buf, w, q, 2 * xl + other), q, 3, 5, sib).wait_recv()
        ag_copy(n, block(buf, w, q, 2 * xr + other), q, 5, 6, sib).wait_recv()
        ag_copy(n, block(buf, w, q, 2 * xo + other, 0), q, 7, 7, sib).wait_recv()
        ag_copy(n, block(buf, w, q, 2 * xo + other, 1), q, 8, 8, sib).wait_recv()

    def ag_drain(n, buf, w, q):
        whole, part = block(buf, w, q, t), block(buf, w, q, t, 0)
        for i in range(9):
            ref = part if i in (4, 6, 7, 8) else whole
            ag_copy(n, ref, q, i, 0, sib).wait_send()

    order = (xo, xr, xl, x)
    rs_refs = (rs0, rs1)

    def rs_copy(src, dst, n, q, i, where):
        return remote(rs_refs[n].at[q, src], rs_refs[n].at[q, dst], rs_send.at[n, q, i], rs_recv.at[n, q, i], where)

    def sib_copy(n, q):
        return rs_copy(slice(0, 4), slice(4, 8), n, q, 0, sib)

    def opp_copy(n, q, i):
        part = pl.ds(i * half, half)
        return remote(
            rs_refs[n].at[q, 8, part],
            rs_refs[n].at[q, 9, part],
            rs_send.at[n, q, 1 + i],
            rs_recv.at[n, q, 1 + i],
            x_right if i == 0 else x_left,
        )

    def nb_copy(n, q, i):
        return rs_copy(10 + i, 12 + i, n, q, 3 + i, x_right if i == 0 else x_left)

    def rs_partials(n, q):
        buf = rs_refs[n]
        width_k = units if n == 0 else 2 * units
        k_range = pl.ds(pl.multiple_of(mine * units, LANES), units) if n == 0 else slice(None)
        h = hid[q * rows : (q + 1) * rows, 0:width_k]
        for k in range(4):
            buf[q, k] = jnp.dot(h, wd[2 * order[k] + other, k_range, :], preferred_element_type=F32).astype(BF16)
        sib_copy(n, q).start()
        for k in range(4):
            acc[q, k] = jnp.dot(h, wd[2 * order[k] + core, k_range, :], preferred_element_type=F32)

    def rs_opposite(n, q):
        buf = rs_refs[n]
        sib_copy(n, q).wait_recv()
        buf[q, 8] = (acc[q, 0] + buf[q, 4].astype(F32)).astype(BF16)
        opp_copy(n, q, 0).start()
        opp_copy(n, q, 1).start()

    def rs_neighbours(n, q):
        buf = rs_refs[n]
        for i in range(2):
            opp_copy(n, q, i).wait_recv()
            near, far = pl.ds(i * half, half), pl.ds((1 - i) * half, half)
            buf[q, 10 + i, near] = (
                acc[q, 1 + i, near] + buf[q, 5 + i, near].astype(F32) + buf[q, 9, near].astype(F32)
            ).astype(BF16)
            buf[q, 10 + i, far] = (acc[q, 1 + i, far] + buf[q, 5 + i, far].astype(F32)).astype(BF16)
            nb_copy(n, q, i).start()

    def rs_total(n, q):
        buf = rs_refs[n]
        nb_copy(n, q, 0).wait_recv()
        nb_copy(n, q, 1).wait_recv()
        return acc[q, 3] + buf[q, 7].astype(F32) + buf[q, 12].astype(F32) + buf[q, 13].astype(F32)

    def rs_drain(n, q):
        sib_copy(n, q).wait_send()
        for i in range(2):
            opp_copy(n, q, i).wait_send()
            nb_copy(n, q, i).wait_send()

    def norm_rows(buf, q, r, base):
        @pl.loop(0, rows // 16, unroll=4)
        def _(i):
            rws = pl.ds(pl.multiple_of(i * 16, 16), 16)
            v = buf[q, rws, :].astype(F32)
            inverse = lax.rsqrt(jnp.sum(v * v, axis=1, keepdims=True) / feat + EPS)
            ub[pl.ds(pl.multiple_of(base + i * 16, 16), 16), :] = (v * inverse * gf[r : r + 1, :]).astype(BF16)

    def hidden_rows(lo, count, columns, n_pairs):
        r = jnp.dot(ub[lo : lo + count, :], gu[:, columns], preferred_element_type=F32)
        for n in range(n_pairs):
            a, b = r[:, 2 * n * LANES : (2 * n + 1) * LANES], r[:, (2 * n + 1) * LANES : (2 * n + 2) * LANES]
            hid[lo : lo + count, n * LANES : (n + 1) * LANES] = (jax.nn.silu(a) * b).astype(BF16)

    def conv(q):
        r = jnp.dot(ub[q * rows : (q + 1) * rows, :], vm[:, : 2 * chan_w], preferred_element_type=F32)
        glued = r[:, :chan_w] * jax.nn.sigmoid(r[:, chan_w:])
        for i in range(rows // LEN):
            pad[i, 32:, :] = glued[i * LEN : (i + 1) * LEN]
        n_taps = taps_in.shape[0]
        taps = taps_in[...].astype(F32)
        for i in range(rows // LEN):
            total = jnp.zeros((LEN, chan_w), F32)
            for k in range(n_taps):
                total = total + taps[k : k + 1, :] * pad[i, 33 - n_taps + k : 33 - n_taps + k + LEN, :]
            cvb[q, i * LEN : (i + 1) * LEN, pl.ds(pl.multiple_of(t * chan_w, chan_w), chan_w)] = total.astype(BF16)

    def channel_norm(q):
        @pl.loop(0, rows // 16, unroll=4)
        def _(i):
            rws = pl.ds(pl.multiple_of(i * 16, 16), 16)
            v = cvb[q, rws, :].astype(F32)
            mu = jnp.sum(v, axis=1, keepdims=True) / chan
            msq = jnp.sum(v * v, axis=1, keepdims=True) / chan
            w = (v - mu) * lax.rsqrt(msq - mu * mu + EPS) * cgb[3:4, :] + cgb[11:12, :]
            mixed[rws, :] = jax.nn.silu(w).astype(BF16)

    def own_cols(buf, q):
        return buf[q, :, own_w]

    def z_begin(kinds):
        for share in range(2):
            for way in range(2):
                for kind in kinds:
                    z_copy(kind, way, share, 1).start()

    def phase(name):
        return jax.named_scope(name)

    chunks = range(nq)
    z_begin((0, 1))
    for q in chunks:
        stream_copy(q).start()
    pl.loop(nq, 2 * nq)(lambda q: ag_start(0, sb0, width, q))

    def pk_copy(i):
        return remote(pk.at[t], pk.at[t], pk_send.at[i - 1], pk_recv.at[t], {"tp": lax.rem(t + i, n_tp)})

    for i in range(1, n_tp):
        pk_copy(i).start()
    spread_mix(z)
    pad[:, :32, :] = jnp.zeros((pad.shape[0], 32, chan_w), F32)

    def theirs_first(fn):
        pl.loop(0, nq)(fn)

    def ours(fn):
        pl.loop(nq, 2 * nq)(fn)

    with phase("w1"):
        relay((0, 1), 1, None)
    with phase("ag0"):
        for q in chunks:
            stream_copy(q).wait_recv()
        theirs_first(lambda q: ag_start(0, sb0, width, q))
        ours(lambda q: ag_relay(0, sb0, width, q))
    with phase("w2"):
        relay((0, 1), 2, None)
    theirs_first(lambda q: ag_relay(0, sb0, width, q))
    ours(lambda q: ag_opposite(0, sb0, width, q))
    with phase("w3"):
        relay((0, 1), 3, None)
    theirs_first(lambda q: ag_opposite(0, sb0, width, q))
    ours(lambda q: ag_end(0, sb0, width, q))
    for i in range(1, n_tp):
        b = lax.rem(t + i, n_tp)
        remote(pk.at[b], pk.at[b], pk_send.at[i - 1], pk_recv.at[b], {"tp": b}).wait_recv()
    for b in range(n_tp):
        gf[:, b * width : (b + 1) * width] = pk[b]
        cgb[0:8, b * chan_w : (b + 1) * chan_w] = pk[b][:, :chan_w]
        cgb[8:16, b * chan_w : (b + 1) * chan_w] = pk[b][:, chan_w : 2 * chan_w]
    with phase("w4"):
        relay((0, 1), 4, None)
    theirs_first(lambda q: ag_end(0, sb0, width, q))
    ours(lambda q: norm_rows(sb0, q, 0, q * rows))
    with phase("w5"):
        relay((0, 1), 5, None)
    theirs_first(lambda q: norm_rows(sb0, q, 0, q * rows))
    with phase("w67"):
        relay((0, 1), 6, None)
        relay((0, 1), 7, None)
    z_begin((2,))
    with phase("w8"):
        relay((0, 1), 8, None)

    late = [((2,), 1), ((2,), 2), ((2,), 3), ((2,), 4), ((2,), 5), ((2,), 6), ((2, 3), 7), ((2, 3), 8)]
    late += [((3,), i) for i in range(3, steps + 1)]

    def background(count=1):
        for _ in range(count):
            kinds, i = late.pop(0)
            with phase(f"late{i}"):
                for kind in kinds:
                    relay((kind,), i - 6 if (kind == 3 and len(kinds) == 2) else i, None)
            if kinds == (2,) and i == 6:
                z_begin((3,))

    tokens = nq * rows
    my_half = pl.ds(pl.multiple_of(mine * 2 * units, LANES), 2 * units)
    with phase("hid_theirs"):
        hidden_rows(0, tokens, my_half, pairs)
    with phase("part_theirs"):
        for q in chunks:
            rs_partials(0, q)
    background()
    with phase("hid_ours"):
        hidden_rows(tokens, tokens, my_half, pairs)
    with phase("rs_a"):
        rs_opposite(0, 0)
        rs_opposite(0, 1)
        rs_partials(0, nq)
        rs_opposite(0, 2)
        rs_neighbours(0, 0)
        rs_partials(0, nq + 1)
    background()

    def pass_over(q):
        ybo[q] = rs_total(0, q).astype(BF16)
        part_copy(q).start()

    with phase("rs_b"):
        rs_neighbours(0, 1)
        rs_partials(0, nq + 2)
        rs_neighbours(0, 2)
        rs_opposite(0, 3)
    background()
    with phase("rs_c"):
        pass_over(0)
        rs_opposite(0, 4)
        pass_over(1)
        rs_neighbours(0, 3)
        rs_opposite(0, 5)
        pass_over(2)
        pl.loop(1, n_fs)(lambda i: y_late(lax.rem(z + i, n_fs)).start())
    background()
    with phase("rs_d"):
        rs_neighbours(0, 4)
        rs_neighbours(0, 5)

    def first(q):
        total = rs_total(0, nq + q)
        part_copy(q).wait_recv()
        sb1[q, :, own_w] = (own_cols(sb0, nq + q).astype(F32) + 0.5 * (total + ybi[q].astype(F32))).astype(BF16)
        ag_start(1, sb1, width, q)

    with phase("first0"):
        first(0)
    background()
    with phase("first12"):
        first(1)
        first(2)
    background()
    with phase("ag1"):
        ag_relay(1, sb1, width, 0)
        ag_relay(1, sb1, width, 1)
        ag_relay(1, sb1, width, 2)
    background()
    with phase("opp1"):
        ag_opposite(1, sb1, width, 0)
        ag_opposite(1, sb1, width, 1)
    background()

    def conv_stage(q):
        ag_end(1, sb1, width, q)
        norm_rows(sb1, q, 1, q * rows)
        conv(q)
        ag_start(2, cvb, chan_w, q)

    with phase("conv0"):
        conv_stage(0)
    background()
    with phase("conv1"):
        ag_opposite(1, sb1, width, 2)
        conv_stage(1)
    background()
    with phase("conv2"):
        ag_relay(2, cvb, chan_w, 0)
        conv_stage(2)
    background()
    with phase("ag2"):
        ag_relay(2, cvb, chan_w, 1)
        ag_opposite(2, cvb, chan_w, 0)
        ag_relay(2, cvb, chan_w, 2)
        ag_opposite(2, cvb, chan_w, 1)

        @pl.loop(0, n_tp)
        def _(b):
            for i in range(2):
                ref = mxb.at[pl.ds(pl.multiple_of(b * chan_w, chan_w), chan_w), pl.ds(i * LANES, LANES)]
                pltpu.make_async_copy(ref, ref, mx_recv.at[b, i]).wait()

    def mix_stage(q):
        ag_end(2, cvb, chan_w, q)
        channel_norm(q)
        branch = jnp.dot(mixed[...], mxb[...], preferred_element_type=F32)
        sb3[q, :, own_w] = (own_cols(sb1, q).astype(F32) + branch).astype(BF16)
        ag_start(3, sb3, width, q)

    with phase("mix0"):
        mix_stage(0)
    background()
    with phase("mix12"):
        ag_opposite(2, cvb, chan_w, 2)
        mix_stage(1)
        ag_relay(3, sb3, width, 0)
        mix_stage(2)
    background()
    with phase("ag3"):
        ag_relay(3, sb3, width, 1)
        ag_opposite(3, sb3, width, 0)
        ag_relay(3, sb3, width, 2)
        ag_opposite(3, sb3, width, 1)
    background()
    assert not late
    with phase("ywait"):
        for i in range(3):
            y_all(i).wait_recv()

    def ffn_stage(q):
        ag_end(3, sb3, width, q)
        norm_rows(sb3, q, 2, q * rows)
        hidden_rows(q * rows, rows, slice(None), 2 * pairs)
        rs_partials(1, q)

    def last(q):
        total = rs_total(1, q)
        out[q * rows : (q + 1) * rows, :] = (own_cols(sb3, q).astype(F32) + 0.5 * total).astype(BF16)

    with phase("ffn0"):
        ffn_stage(0)
    with phase("ffn1"):
        ag_opposite(3, sb3, width, 2)
        ffn_stage(1)
    with phase("ffn2"):
        rs_opposite(1, 0)
        ffn_stage(2)
    with phase("rs1"):
        rs_opposite(1, 1)
        rs_neighbours(1, 0)
        rs_opposite(1, 2)
        rs_neighbours(1, 1)
    with phase("last"):
        last(0)
        rs_neighbours(1, 2)
        last(1)
        last(2)

    for kind in range(4):
        for way in range(2):
            for share in range(2):
                ref = many(kind, share, reach(way, share))
                remote(ref, ref, z_send.at[kind, way, share], z_recv.at[kind, way, share, 0], z_right).wait_send()
    for i in range(3):
        y_all(i).wait_send()
    for i in range(1, n_tp):
        pk_copy(i).wait_send()
    ref = mxb.at[pl.ds(0, (n_tp - 1) * chan_w), :]
    remote(ref, ref, mx_send.at[0], mx_recv.at[0, 0], sib).wait_send()

    @pl.loop(0, nq)
    def _(q):
        stream_copy(q).wait_send()
        part_copy(q).wait_send()
        for n, buf, w in ((0, sb0, width), (1, sb1, width), (2, cvb, chan_w), (3, sb3, width)):
            ag_drain(n, buf, w, q)
        ag_drain(0, sb0, width, nq + q)
        rs_drain(0, q)
        rs_drain(0, nq + q)
        rs_drain(1, q)


def solution(mesh):
    n_fs, n_tp = mesh.shape["fs"], mesh.shape["tp"]

    def local(
        stream_in,
        gain_before,
        gain_mixer,
        gain_after,
        w_gate,
        w_upward,
        w_down,
        w_value,
        w_glu_gate,
        conv_taps,
        chan_gain,
        chan_bias,
        w_mix_out,
    ):
        tokens, width = stream_in.shape
        k_rows, hidden = w_gate.shape
        chan_w = w_value.shape[1]
        units = -(-(hidden // 2) // LANES) * LANES
        nq = CHUNKS
        rows = tokens // nq
        feat, chan = width * n_tp, chan_w * n_tp
        vmem = pltpu.VMEM
        dma = pltpu.SemaphoreType.DMA
        any_space = pl.BlockSpec(memory_space=pl.ANY)
        in_vmem = pl.BlockSpec(memory_space=pltpu.VMEM)
        return pl.pallas_call(
            lambda *refs: layer_kernel(n_fs, n_tp, *refs),
            out_shape=jax.ShapeDtypeStruct((tokens, width), BF16),
            in_specs=[any_space, in_vmem, in_vmem] + [any_space] * 4 + [in_vmem] * 6,
            out_specs=in_vmem,
            scratch_shapes=[
                vmem((n_fs * k_rows, 4 * units), BF16),
                vmem((n_fs // 2, 2 * units, 2 * LANES), BF16),
                vmem((n_fs * k_rows, 3 * chan_w), BF16),
                vmem((chan, 2 * LANES), BF16),
                vmem((n_tp, 8, width), F32),
                vmem((8, feat), F32),
                vmem((16, chan), F32),
                vmem((2 * nq, rows, feat), BF16),
                vmem((nq, rows, feat), BF16),
                vmem((nq, rows, feat), BF16),
                vmem((nq, rows, chan), BF16),
                vmem((2 * tokens, feat), BF16),
                vmem((rows, chan), BF16),
                vmem((2 * tokens, 2 * units), BF16),
                vmem((rows // LEN, LEN + 32, chan_w), F32),
                vmem((nq, rows, width), BF16),
                vmem((nq, rows, width), BF16),
                vmem((2 * nq, 4, rows, width), F32),
                vmem((2 * nq, 14, rows, width), BF16),
                vmem((nq, 14, rows, width), BF16),
                dma((5 + nq,)),
                dma((4, 2, 2, n_fs // 2)),
                dma((4, 2, 2)),
                dma((3,)),
                dma((3,)),
                dma((n_tp,)),
                dma((n_tp - 1,)),
                dma((n_tp, 2)),
                dma((1,)),
                dma((4, 2 * nq, 9)),
                dma((4, 2 * nq, 9)),
                dma((2, 2 * nq, 5)),
                dma((2, 2 * nq, 5)),
                dma((2, nq)),
                dma((2, nq)),
            ],
            compiler_params=pltpu.CompilerParams(
                collective_id=0, has_side_effects=True, vmem_limit_bytes=60 * 1024 * 1024
            ),
        )(
            stream_in,
            w_gate.T,
            w_upward.T,
            w_down,
            w_value,
            w_glu_gate,
            w_mix_out,
            conv_taps,
            gain_before,
            gain_mixer,
            gain_after,
            chan_gain,
            chan_bias,
        )

    in_specs = (
        P(("grp", "fs"), "tp"),
        P("tp"),
        P("tp"),
        P("tp"),
        P("fs", "tp"),
        P("fs", "tp"),
        P("tp", "fs"),
        P("fs", "tp"),
        P("fs", "tp"),
        P(None, "tp"),
        P("tp"),
        P("tp"),
        P("tp", "fs"),
    )
    out_specs = P(("grp", "fs"), "tp")
    return jax.shard_map(local, mesh=mesh, in_specs=in_specs, out_specs=out_specs, check_vma=False)
```

time: 172 us -> 162 us (0.942)
  Pallas kernels: 170 us -> 159 us
    pallas_call x1, Pallas kernels: 170 us -> 159 us  [local(): pl.pallas_call(lambda *refs: layer_kernel(n_fs, n_tp, *refs), out_shape=j...]
where the time goes in v3:
time: 162 us; the launch traced here: 161 us
  Pallas kernels  159 us (98%)
  local copies, waits for them, and re-layouts  1.62 us (1%)
    pallas_call x1, Pallas kernels, local(): pl.pallas_call(lambda *refs: layer_kernel(n_fs, n_tp, *refs), out_shape=j...  159 us

profile of v3, /device:TPU:33, one launch (start us, length us, event | category | flops | bytes accessed | tf_op | source)
XLA Modules:
  0.0 160.9 jit_solution(2896904356087936821)
XLA Ops:
  0.0 159.2 %shard_map.127 = bf16[384,256]{1,0:T(8,128)(2,1)} custom-call(bf16[384,256]{1,0:T(8,128)(2,1)} %refs_0_.1, bf16[704,128]{1,0:T(8,128)(2,1)} %bitcast.2, bf16[704,128]{1,0:T(8,128)(2,1)} %bitcast.3, bf16[704,128]{1,0:T(8,128)(2,1)} %refs_3_.1, bf16[128,128]{1,0:T(8,128)(2,1)} %refs_4_.1, bf16[128,128]{1,0:T(8,128)(2,1)} %refs_5_.1, bf16[128,128]{1,0:T(8,128)(2,1)} %refs_6_.1, ...), custom_call_target="tpu_custom_call" | custom-call | tf_op jit(solution)/shard_map/pallas_call | solution.py:679
  159.2 1.6 %copy.15 = bf16[384,256]{1,0:T(8,128)(2,1)} copy(bf16[384,256]{1,0:T(8,128)(2,1)} %shard_map.127) | data formatting | bytes 393216

commit v4 on v3

v4 whole, which is shorter than its diff:
```python
import jax
import jax.numpy as jnp
from jax import lax
from jax.experimental import pallas as pl
from jax.experimental.pallas import tpu as pltpu
from jax.sharding import PartitionSpec as P

MESH = pl.DeviceIdType.MESH
LEN = 128
EPS = 1e-06
LANES = 128
CHUNKS = 3
BF16, F32 = jnp.bfloat16, jnp.float32


def remote(src, dst, send_sem, recv_sem, where):
    return pltpu.make_async_remote_copy(
        src_ref=src,
        dst_ref=dst,
        send_sem=send_sem,
        recv_sem=recv_sem,
        device_id=where,
        device_id_type=MESH,
    )


def layer_kernel(
    n_fs,
    n_tp,
    s_in,
    gate_in,
    up_in,
    wd_in,
    value_in,
    glu_in,
    mix_in,
    taps_in,
    before_in,
    mixer_in,
    after_in,
    cgain_in,
    cbias_in,
    out,
    gu,
    wd,
    vm,
    mxb,
    pk,
    gf,
    cgb,
    sb0,
    sb1,
    sb3,
    cvb,
    ub,
    mixed,
    hid,
    pad,
    ybo,
    ybi,
    acc,
    rs0,
    rs1,
    load_sem,
    z_recv,
    z_send,
    y_recv,
    y_send,
    pk_recv,
    pk_send,
    mx_recv,
    mx_send,
    ag_recv,
    ag_send,
    rs_recv,
    rs_send,
    yx_recv,
    yx_send,
):
    z, t, g = lax.axis_index("fs"), lax.axis_index("tp"), lax.axis_index("grp")
    parity = lax.rem(g, 2)
    partner = {"grp": g + 1 - 2 * parity}
    z_right = {"fs": lax.rem(z + 1, n_fs)}
    z_left = {"fs": lax.rem(z + n_fs - 1, n_fs)}
    chips = n_tp // 2
    x, core = t // 2, lax.rem(t, 2)
    xr, xl, xo = lax.rem(x + 1, chips), lax.rem(x + 3, chips), lax.rem(x + 2, chips)
    other = 1 - core
    sib = {"tp": 2 * x + other}
    x_right, x_left = {"tp": 2 * xr + core}, {"tp": 2 * xl + core}

    nq, rows, width = sb1.shape[0], sb1.shape[1], s_in.shape[1]
    half = rows // 2
    feat = width * n_tp
    k_rows, chan_w = value_in.shape
    chan = chan_w * n_tp
    steps = n_fs // 2
    own_units = gate_in.shape[0] // 2
    units = wd.shape[1] // 2
    pairs = units // LANES
    mine, theirs = parity, 1 - parity

    own_k = pl.ds(pl.multiple_of(z * k_rows, k_rows), k_rows)

    own_w = pl.ds(pl.multiple_of(t * width, width), width)

    def own_loads():
        for h in range(2):
            yield pltpu.make_async_copy(
                wd_in.at[h * own_units : (h + 1) * own_units, :],
                wd.at[
                    z // 2,
                    h * units : h * units + own_units,
                    pl.ds(pl.multiple_of(lax.rem(z, 2) * LANES, LANES), LANES),
                ],
                load_sem.at[0],
            )
        for i, ref in enumerate((value_in, glu_in, mix_in)):
            yield pltpu.make_async_copy(ref, vm.at[own_k, i * chan_w : (i + 1) * chan_w], load_sem.at[1])
        for q in range(nq):
            yield pltpu.make_async_copy(
                s_in.at[pl.ds(q * rows, rows), :],
                sb0.at[nq + q, :, pl.ds(pl.multiple_of(t * width, width), width)],
                load_sem.at[2],
            )

    for copy in own_loads():
        copy.start()

    for h in range(2):
        for i in range(pairs):
            lo = h * own_units + i * LANES
            hi = min(lo + LANES, (h + 1) * own_units)
            for j, ref in enumerate((gate_in, up_in)):
                v = ref[lo:hi, :]
                if hi - lo < LANES:
                    v = jnp.concatenate([v, jnp.zeros((LANES - hi + lo, k_rows), BF16)], axis=0)
                c = h * 2 * units + (2 * i + j) * LANES
                gu[own_k, c : c + LANES] = v.T
        wd[:, h * units + own_units : (h + 1) * units, :] = jnp.zeros((wd.shape[0], units - own_units, wd.shape[2]), BF16)
    for i, ref in enumerate((before_in, mixer_in, after_in)):
        pk[t, i : i + 1, :] = ref[...].astype(F32).reshape(1, width)
    pk[t, 3:4, :chan_w] = cgain_in[...].astype(F32).reshape(1, chan_w)
    pk[t, 3:4, chan_w:] = cbias_in[...].astype(F32).reshape(1, chan_w)
    pk[t, 4:8, :] = jnp.zeros((4, width), F32)

    barrier = pltpu.get_barrier_semaphore()
    peers = [z_right, z_left, partner] + [{"tp": lax.rem(t + i, n_tp)} for i in range(1, n_tp)]
    for peer in peers:
        pl.semaphore_signal(barrier, inc=1, device_id=peer, device_id_type=MESH)
    pl.semaphore_wait(barrier, len(peers))

    ref = vm.at[own_k, :]
    pltpu.make_async_copy(wd_in, wd_in, load_sem.at[0]).wait()
    pltpu.make_async_copy(ref, ref, load_sem.at[1]).wait()
    pltpu.make_async_copy(s_in, s_in, load_sem.at[2]).wait()

    wide = 2 * LANES * (pairs - 1)
    A0, A1, B, X, M, D = range(6)

    def piece(kind, f, part=None):
        if kind in (B, D):
            size = own_units if part is None else own_units // 2
            q0 = (mine if kind == B else theirs) * units + (0 if part is None else part * size)
            return wd.at[
                f // 2,
                pl.ds(pl.multiple_of(q0, 16), size),
                pl.ds(pl.multiple_of(lax.rem(f, 2) * LANES, LANES), LANES),
            ]
        size = k_rows if part is None else k_rows // 2
        r0 = pl.ds(pl.multiple_of(f * k_rows + (0 if part is None else part * size), size), size)
        c0 = mine * 2 * units
        if kind == A0:
            return gu.at[r0, pl.ds(pl.multiple_of(c0, LANES), wide)]
        if kind == A1:
            return gu.at[r0, pl.ds(pl.multiple_of(c0 + wide, LANES), 2 * units - wide)]
        if kind == X:
            return vm.at[r0, pl.ds(pl.multiple_of(mine * chan_w, LANES), chan_w)]
        return vm.at[r0, 2 * chan_w : 3 * chan_w]

    def many(kind, count):
        if kind in (B, D):
            if count <= wd.shape[0]:
                return wd.at[0:count, 0:own_units, 0:LANES]
            total = count * own_units // 2
            for a in range(1, wd.shape[0] + 1):
                if total % (16 * a) == 0 and total // a <= wd.shape[1]:
                    return wd.at[0:a, 0 : total // a, :]
        if kind == A0:
            return gu.at[0 : count * k_rows, 0:wide]
        if kind == A1:
            return gu.at[0 : count * k_rows, 0 : 2 * units - wide]
        return vm.at[0 : count * k_rows, 0:chan_w]

    def origin(way, s):
        return lax.rem(z + n_fs - s, n_fs) if way == 0 else lax.rem(z + s, n_fs)

    def z_sem(kind, way, s):
        if kind < X:
            return z_recv.at[(kind * 2 + way) * steps + s - 1]
        return z_recv.at[(2 * X + kind - X) * steps + s - 1]

    def z_copy(kind, way, s_next):
        ref = piece(kind, origin(way, s_next - 1), None if s_next < steps else way)
        return remote(ref, ref, z_send.at[kind], z_sem(kind, way, s_next), z_right if way == 0 else z_left)

    def y_copy(ref, i):
        return remote(ref, ref, y_send.at[i], y_recv.at[i], partner)

    def y_all(i):
        return y_copy(many((A0, A1, X)[i], n_fs - 1), i)

    def stream_copy(q):
        return remote(sb0.at[nq + q, :, own_w], sb0.at[q, :, own_w], yx_send.at[0], yx_recv.at[nq], partner)

    def part_copy(q):
        return remote(ybo.at[q], ybi.at[q], yx_send.at[1], yx_recv.at[q], partner)

    def spread_mix(f):
        dest, b = f // 2, lax.rem(f, 2)
        src = piece(M, f)
        dst = mxb.at[
            pl.ds(pl.multiple_of(t * chan_w, chan_w), chan_w), pl.ds(pl.multiple_of(b * LANES, LANES), LANES)
        ]

        @pl.when(dest != t)
        def _():
            remote(src, dst, mx_send.at[0], mx_recv.at[0], {"tp": dest}).start()

        @pl.when(dest == t)
        def _():
            pltpu.make_async_copy(src, dst, mx_recv.at[0]).start()

    def relay(kind, s):
        for way in range(2):
            part = None if s < steps else way
            if kind < X or way == 0:
                ref = piece(kind, origin(way, s), part) if kind < X else many(kind, 2 if s < steps else 1)
                remote(ref, ref, z_send.at[kind], z_sem(kind, way, s), z_right).wait_recv()
            if s < steps:
                z_copy(kind, way, s + 1).start()
            if kind in (A0, X):
                y_copy(piece(kind, origin(way, s), part), 0 if kind == A0 else 2).start()
            if kind == M and (s < steps or way == 0):
                spread_mix(origin(way, s))

    def block(buf, w, q, b, part=None):
        rws = slice(None) if part is None else pl.ds(part * half, half)
        return buf.at[q, rws, pl.ds(pl.multiple_of(b * w, w), w)]

    def ag_copy(n, ref, slot, i, where):
        return remote(ref, ref, ag_send.at[n], ag_recv.at[slot, i], where)

    def ag_slot(n, q):
        return q // nq if n == 0 else 2 + (n - 1) * nq + q

    def ag_chunks(n, q):
        return slice(q, q + nq) if n == 0 else q

    def ag_start(n, buf, w, q):
        slot, own = ag_slot(n, q), block(buf, w, ag_chunks(n, q), t)
        ag_copy(n, own, slot, 0, x_right).start()
        ag_copy(n, own, slot, 0, x_left).start()
        ag_copy(n, own, slot, 2, sib).start()

    def ag_wait(n, buf, w, q, i, count):
        ag_copy(n, buf.at[ag_chunks(n, q), :, 0 : count * w], ag_slot(n, q), i, sib).wait_recv()

    def ag_relay(n, buf, w, q):
        slot, c = ag_slot(n, q), ag_chunks(n, q)
        b_l, b_r = 2 * xl + core, 2 * xr + core
        ag_wait(n, buf, w, q, 0, 2)
        ag_copy(n, block(buf, w, c, b_l, 0), slot, 1, x_right).start()
        ag_copy(n, block(buf, w, c, b_r, 1), slot, 1, x_left).start()
        ag_copy(n, block(buf, w, c, b_l), slot, 2, sib).start()
        ag_copy(n, block(buf, w, c, b_r), slot, 2, sib).start()

    def ag_opposite(n, buf, w, q):
        ag_wait(n, buf, w, q, 1, 1)
        ag_copy(n, block(buf, w, ag_chunks(n, q), 2 * xo + core), ag_slot(n, q), 2, sib).start()

    def ag_end(n, buf, w, q):
        ag_wait(n, buf, w, q, 2, 4)

    def ag_drain(n, buf, w):
        ag_copy(n, buf.at[:, :, 0 : 7 * w], 0, 0, sib).wait_send()

    order = (xo, xr, xl, x)
    rs_refs = (rs0, rs1)

    def rs_copy(src, dst, n, q, i, where):
        return remote(
            rs_refs[n].at[(q, *src)], rs_refs[n].at[(q, *dst)], rs_send.at[n], rs_recv.at[2 * nq * n + q, i], where
        )

    def sib_copy(n, q):
        return rs_copy((slice(0, 4),), (slice(4, 8),), n, q, 0, sib)

    def opp_copy(n, q, i):
        part = pl.ds(i * half, half)
        return rs_copy((8, part), (9, part), n, q, 1, x_right if i == 0 else x_left)

    def nb_copy(n, q, i):
        return rs_copy((10 + i,), (12 + i,), n, q, 2, x_right if i == 0 else x_left)

    def rs_partials(n, q):
        buf = rs_refs[n]
        width_k = units if n == 0 else 2 * units
        k_range = pl.ds(pl.multiple_of(mine * units, LANES), units) if n == 0 else slice(None)
        h = hid[q * rows : (q + 1) * rows, 0:width_k]
        for k in range(4):
            buf[q, k] = jnp.dot(h, wd[2 * order[k] + other, k_range, :], preferred_element_type=F32).astype(BF16)
        sib_copy(n, q).start()
        for k in range(4):
            acc[q, k] = jnp.dot(h, wd[2 * order[k] + core, k_range, :], preferred_element_type=F32)

    def rs_opposite(n, q):
        buf = rs_refs[n]
        sib_copy(n, q).wait_recv()
        buf[q, 8] = (acc[q, 0] + buf[q, 4].astype(F32)).astype(BF16)
        opp_copy(n, q, 0).start()
        opp_copy(n, q, 1).start()

    def rs_neighbours(n, q):
        buf = rs_refs[n]
        rs_copy((9,), (9,), n, q, 1, sib).wait_recv()
        for i in range(2):
            near, far = pl.ds(i * half, half), pl.ds((1 - i) * half, half)
            buf[q, 10 + i, near] = (
                acc[q, 1 + i, near] + buf[q, 5 + i, near].astype(F32) + buf[q, 9, near].astype(F32)
            ).astype(BF16)
            buf[q, 10 + i, far] = (acc[q, 1 + i, far] + buf[q, 5 + i, far].astype(F32)).astype(BF16)
            nb_copy(n, q, i).start()

    def rs_total(n, q):
        buf = rs_refs[n]
        rs_copy((slice(12, 14),), (slice(12, 14),), n, q, 2, sib).wait_recv()
        return acc[q, 3] + buf[q, 7].astype(F32) + buf[q, 12].astype(F32) + buf[q, 13].astype(F32)

    def rs_drain(n):
        ref = rs_refs[n].at[:, 0:7]
        remote(ref, ref, rs_send.at[n], rs_recv.at[0, 0], sib).wait_send()

    def norm_rows(buf, q, r, base):
        @pl.loop(0, rows // 16, unroll=4)
        def _(i):
            rws = pl.ds(pl.multiple_of(i * 16, 16), 16)
            v = buf[q, rws, :].astype(F32)
            inverse = lax.rsqrt(jnp.sum(v * v, axis=1, keepdims=True) / feat + EPS)
            ub[pl.ds(pl.multiple_of(base + i * 16, 16), 16), :] = (v * inverse * gf[r : r + 1, :]).astype(BF16)

    def hidden_rows(lo, count, columns, n_pairs):
        r = jnp.dot(ub[lo : lo + count, :], gu[:, columns], preferred_element_type=F32)
        for n in range(n_pairs):
            a, b = r[:, 2 * n * LANES : (2 * n + 1) * LANES], r[:, (2 * n + 1) * LANES : (2 * n + 2) * LANES]
            hid[lo : lo + count, n * LANES : (n + 1) * LANES] = (jax.nn.silu(a) * b).astype(BF16)

    def conv(q):
        r = jnp.dot(ub[q * rows : (q + 1) * rows, :], vm[:, : 2 * chan_w], preferred_element_type=F32)
        glued = r[:, :chan_w] * jax.nn.sigmoid(r[:, chan_w:])
        for i in range(rows // LEN):
            pad[i, 32:, :] = glued[i * LEN : (i + 1) * LEN]
        n_taps = taps_in.shape[0]
        taps = taps_in[...].astype(F32)
        for i in range(rows // LEN):
            total = jnp.zeros((LEN, chan_w), F32)
            for k in range(n_taps):
                total = total + taps[k : k + 1, :] * pad[i, 33 - n_taps + k : 33 - n_taps + k + LEN, :]
            cvb[q, i * LEN : (i + 1) * LEN, pl.ds(pl.multiple_of(t * chan_w, chan_w), chan_w)] = total.astype(BF16)

    def channel_norm(q):
        @pl.loop(0, rows // 16, unroll=4)
        def _(i):
            rws = pl.ds(pl.multiple_of(i * 16, 16), 16)
            v = cvb[q, rws, :].astype(F32)
            mu = jnp.sum(v, axis=1, keepdims=True) / chan
            msq = jnp.sum(v * v, axis=1, keepdims=True) / chan
            w = (v - mu) * lax.rsqrt(msq - mu * mu + EPS) * cgb[3:4, :] + cgb[11:12, :]
            mixed[rws, :] = jax.nn.silu(w).astype(BF16)

    def own_cols(buf, q):
        return buf[q, :, own_w]

    def z_begin(kinds):
        for kind in kinds:
            for way in range(2):
                z_copy(kind, way, 1).start()

    def relays(kinds, s):
        for kind in kinds:
            relay(kind, s)

    first_kinds = (A0, A1, B)

    def phase(name):
        return jax.named_scope(name)

    chunks = range(nq)
    z_begin(first_kinds)
    for q in chunks:
        stream_copy(q).start()
    ag_start(0, sb0, width, nq)

    def pk_copy(i):
        return remote(pk.at[t], pk.at[t], pk_send.at[0], pk_recv.at[0], {"tp": lax.rem(t + i, n_tp)})

    pk_all = remote(pk.at[0 : n_tp - 1], pk.at[0 : n_tp - 1], pk_send.at[0], pk_recv.at[0], sib)

    for i in range(1, n_tp):
        pk_copy(i).start()
    spread_mix(z)
    pad[:, :32, :] = jnp.zeros((pad.shape[0], 32, chan_w), F32)

    with phase("w1"):
        relays(first_kinds, 1)
    with phase("ag0"):
        ref = sb0.at[0:nq, :, 0:width]
        remote(ref, ref, yx_send.at[0], yx_recv.at[nq], partner).wait_recv()
        ag_start(0, sb0, width, 0)
        ag_relay(0, sb0, width, nq)
    with phase("w2"):
        relays(first_kinds, 2)
    ag_relay(0, sb0, width, 0)
    ag_opposite(0, sb0, width, nq)
    with phase("w3"):
        relays(first_kinds, 3)
    ag_opposite(0, sb0, width, 0)
    ag_end(0, sb0, width, nq)
    pk_all.wait_recv()
    for b in range(n_tp):
        gf[:, b * width : (b + 1) * width] = pk[b]
        cgb[0:8, b * chan_w : (b + 1) * chan_w] = pk[b][:, :chan_w]
        cgb[8:16, b * chan_w : (b + 1) * chan_w] = pk[b][:, chan_w : 2 * chan_w]
    with phase("w4"):
        relays(first_kinds, 4)
    ag_end(0, sb0, width, 0)
    pl.loop(nq, 2 * nq)(lambda q: norm_rows(sb0, q, 0, q * rows))
    with phase("w5"):
        relays(first_kinds, 5)
    pl.loop(0, nq)(lambda q: norm_rows(sb0, q, 0, q * rows))
    with phase("w67"):
        relays(first_kinds, 6)
        relays(first_kinds, 7)
    z_begin((X,))
    with phase("w8"):
        relays(first_kinds, 8)

    def late(*steps_of):
        with phase("late"):
            for kind, i in steps_of:
                relay(kind, i)

    def y_late(lo, hi):
        @pl.loop(lo, hi)
        def _(i):
            y_copy(piece(A1, lax.rem(z + i, n_fs)), 1).start()

    tokens = nq * rows
    my_half = pl.ds(pl.multiple_of(mine * 2 * units, LANES), 2 * units)
    with phase("hid_theirs"):
        hidden_rows(0, tokens, my_half, pairs)
    with phase("part_theirs"):
        for q in chunks:
            rs_partials(0, q)
    late((X, 1))
    y_late(1, 5)
    with phase("hid_ours"):
        hidden_rows(tokens, tokens, my_half, pairs)
    with phase("rs_a"):
        rs_opposite(0, 0)
        rs_opposite(0, 1)
        rs_partials(0, nq)
        late((X, 2))
        rs_opposite(0, 2)
        rs_neighbours(0, 0)
        rs_partials(0, nq + 1)
    late((X, 3))

    def pass_over(q):
        ybo[q] = rs_total(0, q).astype(BF16)
        part_copy(q).start()

    with phase("rs_b"):
        rs_neighbours(0, 1)
        rs_partials(0, nq + 2)
        rs_neighbours(0, 2)
        rs_opposite(0, 3)
    late((X, 4))
    z_begin((M,))
    with phase("rs_c"):
        pass_over(0)
        rs_opposite(0, 4)
        pass_over(1)
        rs_neighbours(0, 3)
        rs_opposite(0, 5)
        pass_over(2)
    late((X, 5), (M, 1))
    z_begin((D,))
    with phase("rs_d"):
        rs_neighbours(0, 4)
        rs_neighbours(0, 5)

    def first(q):
        total = rs_total(0, nq + q)
        part_copy(q).wait_recv()
        sb1[q, :, own_w] = (own_cols(sb0, nq + q).astype(F32) + 0.5 * (total + ybi[q].astype(F32))).astype(BF16)
        ag_start(1, sb1, width, q)

    with phase("first0"):
        first(0)
    late((X, 6), (M, 2))
    with phase("first12"):
        first(1)
        first(2)
    late((X, 7), (M, 3), (D, 1))
    with phase("ag1"):
        ag_relay(1, sb1, width, 0)
        ag_relay(1, sb1, width, 1)
        ag_relay(1, sb1, width, 2)
    late((X, 8), (M, 4))
    y_late(5, n_fs)
    with phase("opp1"):
        ag_opposite(1, sb1, width, 0)
        ag_opposite(1, sb1, width, 1)
    late((M, 5), (D, 2))

    def conv_stage(q):
        ag_end(1, sb1, width, q)
        norm_rows(sb1, q, 1, q * rows)
        conv(q)
        ag_start(2, cvb, chan_w, q)

    with phase("ywaitx"):
        y_all(2).wait_recv()
    with phase("conv0"):
        conv_stage(0)
    late((M, 6), (D, 3))
    with phase("conv1"):
        ag_opposite(1, sb1, width, 2)
        conv_stage(1)
    late((M, 7), (D, 4))
    with phase("conv2"):
        ag_relay(2, cvb, chan_w, 0)
        conv_stage(2)
    late((M, 8), (D, 5))
    with phase("ag2"):
        ag_relay(2, cvb, chan_w, 1)
        ag_opposite(2, cvb, chan_w, 0)
        ag_relay(2, cvb, chan_w, 2)
        ag_opposite(2, cvb, chan_w, 1)

    def mix_stage(q):
        ag_end(2, cvb, chan_w, q)
        channel_norm(q)
        branch = jnp.dot(mixed[...], mxb[...], preferred_element_type=F32)
        sb3[q, :, own_w] = (own_cols(sb1, q).astype(F32) + branch).astype(BF16)
        ag_start(3, sb3, width, q)

    with phase("mixw"):
        pltpu.make_async_copy(mxb, mxb, mx_recv.at[0]).wait()
    with phase("mix0"):
        mix_stage(0)
    late((D, 6))
    with phase("mix12"):
        ag_opposite(2, cvb, chan_w, 2)
        mix_stage(1)
        ag_relay(3, sb3, width, 0)
        mix_stage(2)
    late((D, 7))
    with phase("ag3"):
        ag_relay(3, sb3, width, 1)
        ag_opposite(3, sb3, width, 0)
        ag_relay(3, sb3, width, 2)
        ag_opposite(3, sb3, width, 1)
    late((D, 8))
    with phase("ywait"):
        for i in range(2):
            y_all(i).wait_recv()

    def ffn_stage(q):
        ag_end(3, sb3, width, q)
        norm_rows(sb3, q, 2, q * rows)
        hidden_rows(q * rows, rows, slice(None), 2 * pairs)
        rs_partials(1, q)

    def last(q):
        total = rs_total(1, q)
        out[q * rows : (q + 1) * rows, :] = (own_cols(sb3, q).astype(F32) + 0.5 * total).astype(BF16)

    with phase("ffn0"):
        ffn_stage(0)
    with phase("ffn1"):
        ag_opposite(3, sb3, width, 2)
        ffn_stage(1)
    with phase("ffn2"):
        rs_opposite(1, 0)
        ffn_stage(2)
    with phase("rs1"):
        rs_opposite(1, 1)
        rs_neighbours(1, 0)
        rs_opposite(1, 2)
        rs_neighbours(1, 1)
    with phase("last"):
        last(0)
        rs_neighbours(1, 2)
        last(1)
        last(2)

    for kind in range(6):
        ref = many(kind, n_fs - 1)
        remote(ref, ref, z_send.at[kind], z_recv.at[0], z_right).wait_send()
    for i in range(3):
        y_all(i).wait_send()
    pk_all.wait_send()
    ref = mxb.at[pl.ds(0, (n_tp - 1) * chan_w), :]
    remote(ref, ref, mx_send.at[0], mx_recv.at[0], sib).wait_send()
    ref = sb0.at[0:nq, :, 0:width]
    remote(ref, ref, yx_send.at[0], yx_recv.at[0], partner).wait_send()
    remote(ybo, ybo, yx_send.at[1], yx_recv.at[0], partner).wait_send()
    for n, buf, w in ((0, sb0, width), (1, sb1, width), (2, cvb, chan_w), (3, sb3, width)):
        ag_drain(n, buf, w)
    for n in range(2):
        rs_drain(n)


def solution(mesh):
    n_fs, n_tp = mesh.shape["fs"], mesh.shape["tp"]

    def local(
        stream_in,
        gain_before,
        gain_mixer,
        gain_after,
        w_gate,
        w_upward,
        w_down,
        w_value,
        w_glu_gate,
        conv_taps,
        chan_gain,
        chan_bias,
        w_mix_out,
    ):
        tokens, width = stream_in.shape
        k_rows, hidden = w_gate.shape
        chan_w = w_value.shape[1]
        units = -(-(hidden // 2) // LANES) * LANES
        nq = CHUNKS
        rows = tokens // nq
        feat, chan = width * n_tp, chan_w * n_tp
        vmem = pltpu.VMEM
        dma = pltpu.SemaphoreType.DMA
        any_space = pl.BlockSpec(memory_space=pl.ANY)
        in_vmem = pl.BlockSpec(memory_space=pltpu.VMEM)
        return pl.pallas_call(
            lambda *refs: layer_kernel(n_fs, n_tp, *refs),
            out_shape=jax.ShapeDtypeStruct((tokens, width), BF16),
            in_specs=[any_space, in_vmem, in_vmem] + [any_space] * 4 + [in_vmem] * 6,
            out_specs=in_vmem,
            scratch_shapes=[
                vmem((n_fs * k_rows, 4 * units), BF16),
                vmem((n_fs // 2, 2 * units, 2 * LANES), BF16),
                vmem((n_fs * k_rows, 3 * chan_w), BF16),
                vmem((chan, 2 * LANES), BF16),
                vmem((n_tp, 8, width), F32),
                vmem((8, feat), F32),
                vmem((16, chan), F32),
                vmem((2 * nq, rows, feat), BF16),
                vmem((nq, rows, feat), BF16),
                vmem((nq, rows, feat), BF16),
                vmem((nq, rows, chan), BF16),
                vmem((2 * tokens, feat), BF16),
                vmem((rows, chan), BF16),
                vmem((2 * tokens, 2 * units), BF16),
                vmem((rows // LEN, LEN + 32, chan_w), F32),
                vmem((nq, rows, width), BF16),
                vmem((nq, rows, width), BF16),
                vmem((2 * nq, 4, rows, width), F32),
                vmem((2 * nq, 14, rows, width), BF16),
                vmem((nq, 14, rows, width), BF16),
                dma((3,)),
                dma((9 * (n_fs // 2),)),
                dma((6,)),
                dma((3,)),
                dma((3,)),
                dma((1,)),
                dma((1,)),
                dma((1,)),
                dma((1,)),
                dma((2 + 3 * nq, 3)),
                dma((4,)),
                dma((3 * nq, 3)),
                dma((2,)),
                dma((nq + 1,)),
                dma((2,)),
            ],
            compiler_params=pltpu.CompilerParams(
                collective_id=0, has_side_effects=True, vmem_limit_bytes=60 * 1024 * 1024
            ),
        )(
            stream_in,
            w_gate.T,
            w_upward.T,
            w_down,
            w_value,
            w_glu_gate,
            w_mix_out,
            conv_taps,
            gain_before,
            gain_mixer,
            gain_after,
            chan_gain,
            chan_bias,
        )

    in_specs = (
        P(("grp", "fs"), "tp"),
        P("tp"),
        P("tp"),
        P("tp"),
        P("fs", "tp"),
        P("fs", "tp"),
        P("tp", "fs"),
        P("fs", "tp"),
        P("fs", "tp"),
        P(None, "tp"),
        P("tp"),
        P("tp"),
        P("tp", "fs"),
    )
    out_specs = P(("grp", "fs"), "tp")
    return jax.shard_map(local, mesh=mesh, in_specs=in_specs, out_specs=out_specs, check_vma=False)
```

time: 162 us -> 157 us (0.969)
  Pallas kernels: 159 us -> 154 us
    pallas_call x1, Pallas kernels: 159 us -> 154 us  [local(): pl.pallas_call(lambda *refs: layer_kernel(n_fs, n_tp, *refs), out_shape=j...]
where the time goes in v4:
time: 157 us; the launch traced here: 156 us
  Pallas kernels  154 us (98%)
  local copies, waits for them, and re-layouts  1.62 us (1%)
    pallas_call x1, Pallas kernels, local(): pl.pallas_call(lambda *refs: layer_kernel(n_fs, n_tp, *refs), out_shape=j...  154 us

profile of v4, /device:TPU:33, one launch (start us, length us, event | category | flops | bytes accessed | tf_op | source)
XLA Modules:
  0.0 156.1 jit_solution(15019723034550779474)
XLA Ops:
  0.0 154.5 %shard_map.127 = bf16[384,256]{1,0:T(8,128)(2,1)} custom-call(bf16[384,256]{1,0:T(8,128)(2,1)} %refs_0_.1, bf16[704,128]{1,0:T(8,128)(2,1)} %bitcast.2, bf16[704,128]{1,0:T(8,128)(2,1)} %bitcast.3, bf16[704,128]{1,0:T(8,128)(2,1)} %refs_3_.1, bf16[128,128]{1,0:T(8,128)(2,1)} %refs_4_.1, bf16[128,128]{1,0:T(8,128)(2,1)} %refs_5_.1, bf16[128,128]{1,0:T(8,128)(2,1)} %refs_6_.1, ...), custom_call_target="tpu_custom_call" | custom-call | tf_op jit(solution)/shard_map/pallas_call | solution.py:655
  154.5 1.6 %copy.15 = bf16[384,256]{1,0:T(8,128)(2,1)} copy(bf16[384,256]{1,0:T(8,128)(2,1)} %shard_map.127) | data formatting | bytes 393216

commit v5 on v4

--- a/solution.py
+++ b/solution.py
@@ -76,12 +76,14 @@
     rs_send,
     yx_recv,
     yx_send,
+    part,
 ):
     z, t, g = lax.axis_index("fs"), lax.axis_index("tp"), lax.axis_index("grp")
     parity = lax.rem(g, 2)
     partner = {"grp": g + 1 - 2 * parity}
     z_right = {"fs": lax.rem(z + 1, n_fs)}
     z_left = {"fs": lax.rem(z + n_fs - 1, n_fs)}
+    z_two = ({"fs": lax.rem(z + 2, n_fs)}, {"fs": lax.rem(z + n_fs - 2, n_fs)})
     chips = n_tp // 2
     x, core = t // 2, lax.rem(t, 2)
     xr, xl, xo = lax.rem(x + 1, chips), lax.rem(x + 3, chips), lax.rem(x + 2, chips)
@@ -145,7 +147,7 @@
     pk[t, 4:8, :] = jnp.zeros((4, width), F32)
 
     barrier = pltpu.get_barrier_semaphore()
-    peers = [z_right, z_left, partner] + [{"tp": lax.rem(t + i, n_tp)} for i in range(1, n_tp)]
+    peers = [z_right, z_left, *z_two, partner] + [{"tp": lax.rem(t + i, n_tp)} for i in range(1, n_tp)]
     for peer in peers:
         pl.semaphore_signal(barrier, inc=1, device_id=peer, device_id_type=MESH)
     pl.semaphore_wait(barrier, len(peers))
@@ -196,9 +198,7 @@
         return lax.rem(z + n_fs - s, n_fs) if way == 0 else lax.rem(z + s, n_fs)
 
     def z_sem(kind, way, s):
-        if kind < X:
-            return z_recv.at[(kind * 2 + way) * steps + s - 1]
-        return z_recv.at[(2 * X + kind - X) * steps + s - 1]
+        return z_recv.at[(kind * 2 + way) * steps + s - 1]
 
     def z_copy(kind, way, s_next):
         ref = piece(kind, origin(way, s_next - 1), None if s_next < steps else way)
@@ -234,15 +234,36 @@
     def relay(kind, s):
         for way in range(2):
             part = None if s < steps else way
-            if kind < X or way == 0:
-                ref = piece(kind, origin(way, s), part) if kind < X else many(kind, 2 if s < steps else 1)
-                remote(ref, ref, z_send.at[kind], z_sem(kind, way, s), z_right).wait_recv()
+            ref = piece(kind, origin(way, s), part)
+            remote(ref, ref, z_send.at[kind], z_sem(kind, way, s), z_right).wait_recv()
             if s < steps:
                 z_copy(kind, way, s + 1).start()
-            if kind in (A0, X):
-                y_copy(piece(kind, origin(way, s), part), 0 if kind == A0 else 2).start()
-            if kind == M and (s < steps or way == 0):
-                spread_mix(origin(way, s))
+            if kind == A0:
+                y_copy(ref, 0).start()
+
+    def leap_sem(kind, k):
+        return z_recv.at[2 * X * steps + (kind - X) * (steps // 2) + k - 1]
+
+    def leap_send(kind, k):
+        for far in (True, False):
+            for way in range(2):
+                part = way if far and 2 * k == steps else None
+                ref = piece(kind, origin(way, 2 * k - 2), part)
+                where = z_two[way] if far else (z_right, z_left)[way]
+                remote(ref, ref, z_send.at[kind], leap_sem(kind, k), where).start()
+
+    def leap(kind, k):
+        ref = many(kind, 4 if 2 * k < steps else 3)
+        remote(ref, ref, z_send.at[kind], leap_sem(kind, k), z_right).wait_recv()
+        if 2 * k < steps:
+            leap_send(kind, k + 1)
+        for way, d in ((0, 2 * k), (1, 2 * k), (0, 2 * k - 1), (1, 2 * k - 1)):
+            if d == steps and way == 1:
+                continue
+            if kind == X:
+                y_copy(piece(X, origin(way, d)), 2).start()
+            if kind == M:
+                spread_mix(origin(way, d))
 
     def block(buf, w, q, b, part=None):
         rws = slice(None) if part is None else pl.ds(part * half, half)
@@ -349,11 +370,32 @@
             inverse = lax.rsqrt(jnp.sum(v * v, axis=1, keepdims=True) / feat + EPS)
             ub[pl.ds(pl.multiple_of(base + i * 16, 16), 16), :] = (v * inverse * gf[r : r + 1, :]).astype(BF16)
 
+    def gate_up(a, b):
+        return (jax.nn.silu(a) * b).astype(BF16)
+
     def hidden_rows(lo, count, columns, n_pairs):
         r = jnp.dot(ub[lo : lo + count, :], gu[:, columns], preferred_element_type=F32)
         for n in range(n_pairs):
             a, b = r[:, 2 * n * LANES : (2 * n + 1) * LANES], r[:, (2 * n + 1) * LANES : (2 * n + 2) * LANES]
-            hid[lo : lo + count, n * LANES : (n + 1) * LANES] = (jax.nn.silu(a) * b).astype(BF16)
+            hid[lo : lo + count, n * LANES : (n + 1) * LANES] = gate_up(a, b)
+
+    my_half = pl.ds(pl.multiple_of(mine * 2 * units, LANES), 2 * units)
+
+    def pair_sum(s, lo, count):
+        up = lax.rem(z + s, 2) == 1
+        f = jnp.where(up, lax.rem(z + s - 1, n_fs), lax.rem(z + n_fs - s, n_fs))
+        ks = pl.ds(pl.multiple_of(f // 2 * (2 * k_rows), 2 * k_rows), 2 * k_rows)
+        return jnp.dot(ub[lo : lo + count, ks], gu[ks, my_half], preferred_element_type=F32)
+
+    def gather_pair(s, lo, count):
+        r = pair_sum(s, lo, count)
+        part[lo : lo + count, :] = r if s == 1 else part[lo : lo + count, :] + r
+
+    def last_pair(lo, count):
+        r = part[lo : lo + count, :] + pair_sum(steps, lo, count)
+        for n in range(pairs):
+            a, b = r[:, 2 * n * LANES : (2 * n + 1) * LANES], r[:, (2 * n + 1) * LANES : (2 * n + 2) * LANES]
+            hid[lo : lo + count, n * LANES : (n + 1) * LANES] = gate_up(a, b)
 
     def conv(q):
         r = jnp.dot(ub[q * rows : (q + 1) * rows, :], vm[:, : 2 * chan_w], preferred_element_type=F32)
@@ -431,50 +473,59 @@
         gf[:, b * width : (b + 1) * width] = pk[b]
         cgb[0:8, b * chan_w : (b + 1) * chan_w] = pk[b][:, :chan_w]
         cgb[8:16, b * chan_w : (b + 1) * chan_w] = pk[b][:, chan_w : 2 * chan_w]
+    tokens = nq * rows
+    pl.loop(nq, 2 * nq)(lambda q: norm_rows(sb0, q, 0, q * rows))
     with phase("w4"):
         relays(first_kinds, 4)
     ag_end(0, sb0, width, 0)
-    pl.loop(nq, 2 * nq)(lambda q: norm_rows(sb0, q, 0, q * rows))
+    pl.loop(0, nq)(lambda q: norm_rows(sb0, q, 0, q * rows))
+
+    def relay_and_sum(s, work):
+        for kind, some in zip(first_kinds, work):
+            relay(kind, s)
+            for i, lo in some:
+                gather_pair(i, lo, tokens)
+
     with phase("w5"):
-        relays(first_kinds, 5)
-    pl.loop(0, nq)(lambda q: norm_rows(sb0, q, 0, q * rows))
-    with phase("w67"):
-        relays(first_kinds, 6)
-        relays(first_kinds, 7)
-    z_begin((X,))
+        relay_and_sum(5, (((1, 0),), ((1, tokens),), ((2, 0), (2, tokens))))
+    with phase("w6"):
+        relay_and_sum(6, (((3, 0),), ((3, tokens),), ((4, 0), (4, tokens))))
+    with phase("w7"):
+        relay_and_sum(7, (((5, 0),), ((5, tokens), (6, 0)), ((6, tokens), (7, 0), (7, tokens))))
+    leap_send(X, 1)
     with phase("w8"):
-        relays(first_kinds, 8)
+        relays((A0, A1), 8)
 
     def late(*steps_of):
         with phase("late"):
             for kind, i in steps_of:
-                relay(kind, i)
+                leap(kind, i)
 
     def y_late(lo, hi):
         @pl.loop(lo, hi)
         def _(i):
             y_copy(piece(A1, lax.rem(z + i, n_fs)), 1).start()
 
-    tokens = nq * rows
-    my_half = pl.ds(pl.multiple_of(mine * 2 * units, LANES), 2 * units)
     with phase("hid_theirs"):
-        hidden_rows(0, tokens, my_half, pairs)
+        last_pair(0, tokens)
+    with phase("w8b"):
+        relay(B, 8)
     with phase("part_theirs"):
         for q in chunks:
             rs_partials(0, q)
     late((X, 1))
     y_late(1, 5)
     with phase("hid_ours"):
-        hidden_rows(tokens, tokens, my_half, pairs)
+        last_pair(tokens, tokens)
     with phase("rs_a"):
         rs_opposite(0, 0)
         rs_opposite(0, 1)
         rs_partials(0, nq)
-        late((X, 2))
         rs_opposite(0, 2)
         rs_neighbours(0, 0)
         rs_partials(0, nq + 1)
-    late((X, 3))
+    late((X, 2))
+    leap_send(M, 1)
 
     def pass_over(q):
         ybo[q] = rs_total(0, q).astype(BF16)
@@ -485,8 +536,6 @@
         rs_partials(0, nq + 2)
         rs_neighbours(0, 2)
         rs_opposite(0, 3)
-    late((X, 4))
-    z_begin((M,))
     with phase("rs_c"):
         pass_over(0)
         rs_opposite(0, 4)
@@ -494,8 +543,7 @@
         rs_neighbours(0, 3)
         rs_opposite(0, 5)
         pass_over(2)
-    late((X, 5), (M, 1))
-    z_begin((D,))
+    late((X, 3), (M, 1))
     with phase("rs_d"):
         rs_neighbours(0, 4)
         rs_neighbours(0, 5)
@@ -508,21 +556,21 @@
 
     with phase("first0"):
         first(0)
-    late((X, 6), (M, 2))
+    late((X, 4))
+    leap_send(D, 1)
     with phase("first12"):
         first(1)
         first(2)
-    late((X, 7), (M, 3), (D, 1))
+    late((M, 2), (D, 1))
+    y_late(5, n_fs)
     with phase("ag1"):
         ag_relay(1, sb1, width, 0)
         ag_relay(1, sb1, width, 1)
         ag_relay(1, sb1, width, 2)
-    late((X, 8), (M, 4))
-    y_late(5, n_fs)
     with phase("opp1"):
         ag_opposite(1, sb1, width, 0)
         ag_opposite(1, sb1, width, 1)
-    late((M, 5), (D, 2))
+    late((M, 3), (D, 2))
 
     def conv_stage(q):
         ag_end(1, sb1, width, q)
@@ -534,15 +582,14 @@
         y_all(2).wait_recv()
     with phase("conv0"):
         conv_stage(0)
-    late((M, 6), (D, 3))
     with phase("conv1"):
         ag_opposite(1, sb1, width, 2)
         conv_stage(1)
-    late((M, 7), (D, 4))
+    late((M, 4))
     with phase("conv2"):
         ag_relay(2, cvb, chan_w, 0)
         conv_stage(2)
-    late((M, 8), (D, 5))
+    late((D, 3))
     with phase("ag2"):
         ag_relay(2, cvb, chan_w, 1)
         ag_opposite(2, cvb, chan_w, 0)
@@ -560,19 +607,17 @@
         pltpu.make_async_copy(mxb, mxb, mx_recv.at[0]).wait()
     with phase("mix0"):
         mix_stage(0)
-    late((D, 6))
     with phase("mix12"):
         ag_opposite(2, cvb, chan_w, 2)
         mix_stage(1)
         ag_relay(3, sb3, width, 0)
         mix_stage(2)
-    late((D, 7))
+    late((D, 4))
     with phase("ag3"):
         ag_relay(3, sb3, width, 1)
         ag_opposite(3, sb3, width, 0)
         ag_relay(3, sb3, width, 2)
         ag_opposite(3, sb3, width, 1)
-    late((D, 8))
     with phase("ywait"):
         for i in range(2):
             y_all(i).wait_recv()
@@ -679,7 +724,7 @@
                 vmem((2 * nq, 14, rows, width), BF16),
                 vmem((nq, 14, rows, width), BF16),
                 dma((3,)),
-                dma((9 * (n_fs // 2),)),
+                dma((6 * (n_fs // 2) + 3 * (n_fs // 4),)),
                 dma((6,)),
                 dma((3,)),
                 dma((3,)),
@@ -693,6 +738,7 @@
                 dma((2,)),
                 dma((nq + 1,)),
                 dma((2,)),
+                vmem((2 * tokens, 2 * units), F32),
             ],
             compiler_params=pltpu.CompilerParams(
                 collective_id=0, has_side_effects=True, vmem_limit_bytes=60 * 1024 * 1024

time: 157 us -> 151 us (0.962)
  Pallas kernels: 154 us -> 148 us
    pallas_call x1, Pallas kernels: 154 us -> 148 us  [local(): pl.pallas_call(lambda *refs: layer_kernel(n_fs, n_tp, *refs), out_shape=j...]
where the time goes in v5:
time: 151 us; the launch traced here: 149 us
  Pallas kernels  148 us (98%)
  local copies, waits for them, and re-layouts  1.62 us (1%)
    pallas_call x1, Pallas kernels, local(): pl.pallas_call(lambda *refs: layer_kernel(n_fs, n_tp, *refs), out_shape=j...  148 us

profile of v5, /device:TPU:33, one launch (start us, length us, event | category | flops | bytes accessed | tf_op | source)
XLA Modules:
  0.0 149.4 jit_solution(14822857552781608597)
XLA Ops:
  0.0 147.8 %shard_map.127 = bf16[384,256]{1,0:T(8,128)(2,1)} custom-call(bf16[384,256]{1,0:T(8,128)(2,1)} %refs_0_.1, bf16[704,128]{1,0:T(8,128)(2,1)} %bitcast.2, bf16[704,128]{1,0:T(8,128)(2,1)} %bitcast.3, bf16[704,128]{1,0:T(8,128)(2,1)} %refs_3_.1, bf16[128,128]{1,0:T(8,128)(2,1)} %refs_4_.1, bf16[128,128]{1,0:T(8,128)(2,1)} %refs_5_.1, bf16[128,128]{1,0:T(8,128)(2,1)} %refs_6_.1, ...), custom_call_target="tpu_custom_call" | custom-call | tf_op jit(solution)/shard_map/pallas_call | solution.py:700
  147.8 1.6 %copy.15 = bf16[384,256]{1,0:T(8,128)(2,1)} copy(bf16[384,256]{1,0:T(8,128)(2,1)} %shard_map.127) | data formatting | bytes 393216

commit v6 on v5

--- a/solution.py
+++ b/solution.py
@@ -513,40 +513,15 @@
     with phase("part_theirs"):
         for q in chunks:
             rs_partials(0, q)
-    late((X, 1))
-    y_late(1, 5)
     with phase("hid_ours"):
         last_pair(tokens, tokens)
-    with phase("rs_a"):
-        rs_opposite(0, 0)
-        rs_opposite(0, 1)
-        rs_partials(0, nq)
-        rs_opposite(0, 2)
-        rs_neighbours(0, 0)
-        rs_partials(0, nq + 1)
-    late((X, 2))
+    late((X, 1))
     leap_send(M, 1)
+    y_late(1, 5)
 
     def pass_over(q):
         ybo[q] = rs_total(0, q).astype(BF16)
         part_copy(q).start()
-
-    with phase("rs_b"):
-        rs_neighbours(0, 1)
-        rs_partials(0, nq + 2)
-        rs_neighbours(0, 2)
-        rs_opposite(0, 3)
-    with phase("rs_c"):
-        pass_over(0)
-        rs_opposite(0, 4)
-        pass_over(1)
-        rs_neighbours(0, 3)
-        rs_opposite(0, 5)
-        pass_over(2)
-    late((X, 3), (M, 1))
-    with phase("rs_d"):
-        rs_neighbours(0, 4)
-        rs_neighbours(0, 5)
 
     def first(q):
         total = rs_total(0, nq + q)
@@ -554,23 +529,39 @@
         sb1[q, :, own_w] = (own_cols(sb0, nq + q).astype(F32) + 0.5 * (total + ybi[q].astype(F32))).astype(BF16)
         ag_start(1, sb1, width, q)
 
-    with phase("first0"):
-        first(0)
-    late((X, 4))
+    with phase("rs_a"):
+        for q in chunks:
+            rs_opposite(0, q)
+            rs_partials(0, nq + q)
+        for q in chunks:
+            rs_opposite(0, nq + q)
+    with phase("rs_b"):
+        rs_neighbours(0, 0)
+    late((X, 2), (M, 1))
     leap_send(D, 1)
-    with phase("first12"):
-        first(1)
-        first(2)
-    late((M, 2), (D, 1))
+    with phase("rs_c"):
+        rs_neighbours(0, 1)
+        rs_neighbours(0, 2)
+        rs_neighbours(0, nq)
+        pass_over(0)
+        rs_neighbours(0, nq + 1)
+        pass_over(1)
+    late((X, 3), (M, 2))
+    with phase("rs_d"):
+        rs_neighbours(0, nq + 2)
+        pass_over(2)
+    with phase("first"):
+        for q in chunks:
+            first(q)
+    late((X, 4), (M, 3), (D, 1))
     y_late(5, n_fs)
     with phase("ag1"):
-        ag_relay(1, sb1, width, 0)
-        ag_relay(1, sb1, width, 1)
-        ag_relay(1, sb1, width, 2)
+        for q in chunks:
+            ag_relay(1, sb1, width, q)
+    late((M, 4))
     with phase("opp1"):
         ag_opposite(1, sb1, width, 0)
         ag_opposite(1, sb1, width, 1)
-    late((M, 3), (D, 2))
 
     def conv_stage(q):
         ag_end(1, sb1, width, q)
@@ -582,18 +573,15 @@
         y_all(2).wait_recv()
     with phase("conv0"):
         conv_stage(0)
-    with phase("conv1"):
+    with phase("conv12"):
         ag_opposite(1, sb1, width, 2)
         conv_stage(1)
-    late((M, 4))
-    with phase("conv2"):
-        ag_relay(2, cvb, chan_w, 0)
         conv_stage(2)
-    late((D, 3))
+    late((D, 2))
     with phase("ag2"):
-        ag_relay(2, cvb, chan_w, 1)
+        for q in chunks:
+            ag_relay(2, cvb, chan_w, q)
         ag_opposite(2, cvb, chan_w, 0)
-        ag_relay(2, cvb, chan_w, 2)
         ag_opposite(2, cvb, chan_w, 1)
 
     def mix_stage(q):
@@ -610,14 +598,14 @@
     with phase("mix12"):
         ag_opposite(2, cvb, chan_w, 2)
         mix_stage(1)
-        ag_relay(3, sb3, width, 0)
         mix_stage(2)
+    late((D, 3))
+    with phase("ag3"):
+        for q in chunks:
+            ag_relay(3, sb3, width, q)
+        ag_opposite(3, sb3, width, 0)
+        ag_opposite(3, sb3, width, 1)
     late((D, 4))
-    with phase("ag3"):
-        ag_relay(3, sb3, width, 1)
-        ag_opposite(3, sb3, width, 0)
-        ag_relay(3, sb3, width, 2)
-        ag_opposite(3, sb3, width, 1)
     with phase("ywait"):
         for i in range(2):
             y_all(i).wait_recv()
@@ -642,14 +630,12 @@
         ffn_stage(2)
     with phase("rs1"):
         rs_opposite(1, 1)
-        rs_neighbours(1, 0)
         rs_opposite(1, 2)
-        rs_neighbours(1, 1)
+        for q in chunks:
+            rs_neighbours(1, q)
     with phase("last"):
-        last(0)
-        rs_neighbours(1, 2)
-        last(1)
-        last(2)
+        for q in chunks:
+            last(q)
 
     for kind in range(6):
         ref = many(kind, n_fs - 1)

time: 151 us -> 145 us (0.960)
  Pallas kernels: 148 us -> 143 us
    pallas_call x1, Pallas kernels: 148 us -> 143 us  [local(): pl.pallas_call(lambda *refs: layer_kernel(n_fs, n_tp, *refs), out_shape=j...]
where the time goes in v6:
time: 145 us
  Pallas kernels  143 us (99%)
  local copies, waits for them, and re-layouts  1.62 us (1%)
    pallas_call x1, Pallas kernels, local(): pl.pallas_call(lambda *refs: layer_kernel(n_fs, n_tp, *refs), out_shape=j...  143 us

profile of v6, /device:TPU:33, one launch (start us, length us, event | category | flops | bytes accessed | tf_op | source)
XLA Modules:
  0.0 144.7 jit_solution(11325665006065570107)
XLA Ops:
  0.0 143.0 %shard_map.127 = bf16[384,256]{1,0:T(8,128)(2,1)} custom-call(bf16[384,256]{1,0:T(8,128)(2,1)} %refs_0_.1, bf16[704,128]{1,0:T(8,128)(2,1)} %bitcast.2, bf16[704,128]{1,0:T(8,128)(2,1)} %bitcast.3, bf16[704,128]{1,0:T(8,128)(2,1)} %refs_3_.1, bf16[128,128]{1,0:T(8,128)(2,1)} %refs_4_.1, bf16[128,128]{1,0:T(8,128)(2,1)} %refs_5_.1, bf16[128,128]{1,0:T(8,128)(2,1)} %refs_6_.1, ...), custom_call_target="tpu_custom_call" | custom-call | tf_op jit(solution)/shard_map/pallas_call | solution.py:686
  143.0 1.6 %copy.15 = bf16[384,256]{1,0:T(8,128)(2,1)} copy(bf16[384,256]{1,0:T(8,128)(2,1)} %shard_map.127) | data formatting | bytes 393216

commit v7 on v6

--- a/solution.py
+++ b/solution.py
@@ -77,6 +77,8 @@
     yx_recv,
     yx_send,
     part,
+    g3,
+    shard,
 ):
     z, t, g = lax.axis_index("fs"), lax.axis_index("tp"), lax.axis_index("grp")
     parity = lax.rem(g, 2)
@@ -106,7 +108,17 @@
 
     own_w = pl.ds(pl.multiple_of(t * width, width), width)
 
+    rest = g3.shape[2] // 2
+
     def own_loads():
+        for j, ref in enumerate((gate_in, up_in)):
+            yield pltpu.make_async_copy(ref, shard.at[j], load_sem.at[3])
+            for h in range(2):
+                yield pltpu.make_async_copy(
+                    ref.at[(h + 1) * own_units - rest : (h + 1) * own_units, :],
+                    g3.at[h, z, j * rest : (j + 1) * rest, :],
+                    load_sem.at[4],
+                )
         for h in range(2):
             yield pltpu.make_async_copy(
                 wd_in.at[h * own_units : (h + 1) * own_units, :],
@@ -129,16 +141,26 @@
     for copy in own_loads():
         copy.start()
 
+    barrier = pltpu.get_barrier_semaphore()
+    peers = [z_right, z_left, *z_two, partner] + [{"tp": lax.rem(t + i, n_tp)} for i in range(1, n_tp)]
+    for peer in peers:
+        pl.semaphore_signal(barrier, inc=1, device_id=peer, device_id_type=MESH)
+
+    def unpack(h, f):
+        rws = pl.ds(pl.multiple_of(f * k_rows, k_rows), k_rows)
+        for j in range(2):
+            v = jnp.concatenate([g3[h, f, j * rest : (j + 1) * rest, :], jnp.zeros((LANES - rest, k_rows), BF16)], axis=0)
+            c = pl.multiple_of(h * 2 * units + 2 * units - (2 - j) * LANES, LANES)
+            gu[rws, pl.ds(c, LANES)] = v.T
+
+    pltpu.make_async_copy(shard, shard, load_sem.at[3]).wait()
+    pltpu.make_async_copy(g3.at[:, z], g3.at[:, z], load_sem.at[4]).wait()
     for h in range(2):
-        for i in range(pairs):
-            lo = h * own_units + i * LANES
-            hi = min(lo + LANES, (h + 1) * own_units)
-            for j, ref in enumerate((gate_in, up_in)):
-                v = ref[lo:hi, :]
-                if hi - lo < LANES:
-                    v = jnp.concatenate([v, jnp.zeros((LANES - hi + lo, k_rows), BF16)], axis=0)
-                c = h * 2 * units + (2 * i + j) * LANES
-                gu[own_k, c : c + LANES] = v.T
+        for i in range(pairs - 1):
+            for j in range(2):
+                lo, c = h * own_units + i * LANES, h * 2 * units + (2 * i + j) * LANES
+                gu[own_k, c : c + LANES] = shard[j, lo : lo + LANES, :].T
+        unpack(h, z)
         wd[:, h * units + own_units : (h + 1) * units, :] = jnp.zeros((wd.shape[0], units - own_units, wd.shape[2]), BF16)
     for i, ref in enumerate((before_in, mixer_in, after_in)):
         pk[t, i : i + 1, :] = ref[...].astype(F32).reshape(1, width)
@@ -146,10 +168,6 @@
     pk[t, 3:4, chan_w:] = cbias_in[...].astype(F32).reshape(1, chan_w)
     pk[t, 4:8, :] = jnp.zeros((4, width), F32)
 
-    barrier = pltpu.get_barrier_semaphore()
-    peers = [z_right, z_left, *z_two, partner] + [{"tp": lax.rem(t + i, n_tp)} for i in range(1, n_tp)]
-    for peer in peers:
-        pl.semaphore_signal(barrier, inc=1, device_id=peer, device_id_type=MESH)
     pl.semaphore_wait(barrier, len(peers))
 
     ref = vm.at[own_k, :]
@@ -169,13 +187,13 @@
                 pl.ds(pl.multiple_of(q0, 16), size),
                 pl.ds(pl.multiple_of(lax.rem(f, 2) * LANES, LANES), LANES),
             ]
+        if kind == A1:
+            return g3.at[mine, f] if part is None else g3.at[mine, f, part * rest : (part + 1) * rest]
         size = k_rows if part is None else k_rows // 2
         r0 = pl.ds(pl.multiple_of(f * k_rows + (0 if part is None else part * size), size), size)
         c0 = mine * 2 * units
         if kind == A0:
             return gu.at[r0, pl.ds(pl.multiple_of(c0, LANES), wide)]
-        if kind == A1:
-            return gu.at[r0, pl.ds(pl.multiple_of(c0 + wide, LANES), 2 * units - wide)]
         if kind == X:
             return vm.at[r0, pl.ds(pl.multiple_of(mine * chan_w, LANES), chan_w)]
         return vm.at[r0, 2 * chan_w : 3 * chan_w]
@@ -191,7 +209,7 @@
         if kind == A0:
             return gu.at[0 : count * k_rows, 0:wide]
         if kind == A1:
-            return gu.at[0 : count * k_rows, 0 : 2 * units - wide]
+            return g3.at[0, 0:count]
         return vm.at[0 : count * k_rows, 0:chan_w]
 
     def origin(way, s):
@@ -240,6 +258,8 @@
                 z_copy(kind, way, s + 1).start()
             if kind == A0:
                 y_copy(ref, 0).start()
+            if kind == A1 and (s < steps or way == 1):
+                unpack(mine, origin(way, s))
 
     def leap_sem(kind, k):
         return z_recv.at[2 * X * steps + (kind - X) * (steps // 2) + k - 1]
@@ -581,6 +601,8 @@
     with phase("ag2"):
         for q in chunks:
             ag_relay(2, cvb, chan_w, q)
+        y_all(1).wait_recv()
+        pl.loop(1, n_fs)(lambda i: unpack(theirs, lax.rem(z + i, n_fs)))
         ag_opposite(2, cvb, chan_w, 0)
         ag_opposite(2, cvb, chan_w, 1)
 
@@ -607,8 +629,7 @@
         ag_opposite(3, sb3, width, 1)
     late((D, 4))
     with phase("ywait"):
-        for i in range(2):
-            y_all(i).wait_recv()
+        y_all(0).wait_recv()
 
     def ffn_stage(q):
         ag_end(3, sb3, width, q)
@@ -686,7 +707,7 @@
         return pl.pallas_call(
             lambda *refs: layer_kernel(n_fs, n_tp, *refs),
             out_shape=jax.ShapeDtypeStruct((tokens, width), BF16),
-            in_specs=[any_space, in_vmem, in_vmem] + [any_space] * 4 + [in_vmem] * 6,
+            in_specs=[any_space] * 7 + [in_vmem] * 6,
             out_specs=in_vmem,
             scratch_shapes=[
                 vmem((n_fs * k_rows, 4 * units), BF16),
@@ -709,7 +730,7 @@
                 vmem((2 * nq, 4, rows, width), F32),
                 vmem((2 * nq, 14, rows, width), BF16),
                 vmem((nq, 14, rows, width), BF16),
-                dma((3,)),
+                dma((5,)),
                 dma((6 * (n_fs // 2) + 3 * (n_fs // 4),)),
                 dma((6,)),
                 dma((3,)),
@@ -725,6 +746,8 @@
                 dma((nq + 1,)),
                 dma((2,)),
                 vmem((2 * tokens, 2 * units), F32),
+                vmem((2, n_fs, 2 * ((hidden // 2 - 1) % LANES + 1), k_rows), BF16),
+                vmem((2, hidden, k_rows), BF16),
             ],
             compiler_params=pltpu.CompilerParams(
                 collective_id=0, has_side_effects=True, vmem_limit_bytes=60 * 1024 * 1024

time: 145 us -> 141 us (0.972)
  Pallas kernels: 143 us -> 140 us
    pallas_call x1, Pallas kernels: 143 us -> 140 us  [local(): pl.pallas_call(lambda *refs: layer_kernel(n_fs, n_tp, *refs), out_shape=j...]
where the time goes in v7:
time: 141 us
  Pallas kernels  140 us (99%)
  local copies, waits for them, and re-layouts  1.62 us (1%)
    pallas_call x1, Pallas kernels, local(): pl.pallas_call(lambda *refs: layer_kernel(n_fs, n_tp, *refs), out_shape=j...  140 us

profile of v7, /device:TPU:33, one launch (start us, length us, event | category | flops | bytes accessed | tf_op | source)
XLA Modules:
  0.0 141.3 jit_solution(15158346209391726229)
XLA Ops:
  0.0 139.7 %shard_map.127 = bf16[384,256]{1,0:T(8,128)(2,1)} custom-call(bf16[384,256]{1,0:T(8,128)(2,1)} %refs_0_.1, bf16[704,128]{1,0:T(8,128)(2,1)} %bitcast.2, bf16[704,128]{1,0:T(8,128)(2,1)} %bitcast.3, bf16[704,128]{1,0:T(8,128)(2,1)} %refs_3_.1, bf16[128,128]{1,0:T(8,128)(2,1)} %refs_4_.1, bf16[128,128]{1,0:T(8,128)(2,1)} %refs_5_.1, bf16[128,128]{1,0:T(8,128)(2,1)} %refs_6_.1, ...), custom_call_target="tpu_custom_call" | custom-call | tf_op jit(solution)/shard_map/pallas_call | solution.py:707
  139.7 1.6 %copy.15 = bf16[384,256]{1,0:T(8,128)(2,1)} copy(bf16[384,256]{1,0:T(8,128)(2,1)} %shard_map.127) | data formatting | bytes 393216

commit v8 on v7

--- a/solution.py
+++ b/solution.py
@@ -10,6 +10,7 @@
 EPS = 1e-06
 LANES = 128
 CHUNKS = 3
+Y_ROWS = 160
 BF16, F32 = jnp.bfloat16, jnp.float32
 
 
@@ -176,12 +177,15 @@
     pltpu.make_async_copy(s_in, s_in, load_sem.at[2]).wait()
 
     wide = 2 * LANES * (pairs - 1)
-    A0, A1, B, X, M, D = range(6)
+    A0, A1, B, X, M, D, Y = range(7)
+
+    def down_rows(kind):
+        return {B: own_units, D: own_units - Y_ROWS, Y: Y_ROWS}[kind]
 
     def piece(kind, f, part=None):
-        if kind in (B, D):
-            size = own_units if part is None else own_units // 2
-            q0 = (mine if kind == B else theirs) * units + (0 if part is None else part * size)
+        if kind in (B, D, Y):
+            size = down_rows(kind) if part is None else down_rows(kind) // 2
+            q0 = (theirs * units + Y_ROWS if kind == D else mine * units) + (0 if part is None else part * size)
             return wd.at[
                 f // 2,
                 pl.ds(pl.multiple_of(q0, 16), size),
@@ -199,10 +203,11 @@
         return vm.at[r0, 2 * chan_w : 3 * chan_w]
 
     def many(kind, count):
-        if kind in (B, D):
+        if kind in (B, D, Y):
+            size = down_rows(kind)
             if count <= wd.shape[0]:
-                return wd.at[0:count, 0:own_units, 0:LANES]
-            total = count * own_units // 2
+                return wd.at[0:count, 0:size, 0:LANES]
+            total = count * size // 2
             for a in range(1, wd.shape[0] + 1):
                 if total % (16 * a) == 0 and total // a <= wd.shape[1]:
                     return wd.at[0:a, 0 : total // a, :]
@@ -226,7 +231,7 @@
         return remote(ref, ref, y_send.at[i], y_recv.at[i], partner)
 
     def y_all(i):
-        return y_copy(many((A0, A1, X)[i], n_fs - 1), i)
+        return y_copy(many((A0, A1, X, Y)[i], n_fs - 1), i)
 
     def stream_copy(q):
         return remote(sb0.at[nq + q, :, own_w], sb0.at[q, :, own_w], yx_send.at[0], yx_recv.at[nq], partner)
@@ -537,7 +542,7 @@
         last_pair(tokens, tokens)
     late((X, 1))
     leap_send(M, 1)
-    y_late(1, 5)
+    y_late(1, 8)
 
     def pass_over(q):
         ybo[q] = rs_total(0, q).astype(BF16)
@@ -557,10 +562,10 @@
             rs_opposite(0, nq + q)
     with phase("rs_b"):
         rs_neighbours(0, 0)
+        rs_neighbours(0, 1)
     late((X, 2), (M, 1))
     leap_send(D, 1)
     with phase("rs_c"):
-        rs_neighbours(0, 1)
         rs_neighbours(0, 2)
         rs_neighbours(0, nq)
         pass_over(0)
@@ -574,7 +579,8 @@
         for q in chunks:
             first(q)
     late((X, 4), (M, 3), (D, 1))
-    y_late(5, n_fs)
+    y_late(8, n_fs)
+    pl.loop(1, n_fs)(lambda i: y_copy(piece(Y, lax.rem(z + i, n_fs)), 3).start())
     with phase("ag1"):
         for q in chunks:
             ag_relay(1, sb1, width, q)
@@ -630,6 +636,7 @@
     late((D, 4))
     with phase("ywait"):
         y_all(0).wait_recv()
+        y_all(3).wait_recv()
 
     def ffn_stage(q):
         ag_end(3, sb3, width, q)
@@ -661,7 +668,7 @@
     for kind in range(6):
         ref = many(kind, n_fs - 1)
         remote(ref, ref, z_send.at[kind], z_recv.at[0], z_right).wait_send()
-    for i in range(3):
+    for i in range(4):
         y_all(i).wait_send()
     pk_all.wait_send()
     ref = mxb.at[pl.ds(0, (n_tp - 1) * chan_w), :]
@@ -733,8 +740,8 @@
                 dma((5,)),
                 dma((6 * (n_fs // 2) + 3 * (n_fs // 4),)),
                 dma((6,)),
-                dma((3,)),
-                dma((3,)),
+                dma((4,)),
+                dma((4,)),
                 dma((1,)),
                 dma((1,)),
                 dma((1,)),

time: 141 us -> 142 us (level)
  no operation moved by 1% of the time
where the time goes in v8:
time: 142 us
  Pallas kernels  140 us (99%)
  local copies, waits for them, and re-layouts  1.62 us (1%)
    pallas_call x1, Pallas kernels, local(): pl.pallas_call(lambda *refs: layer_kernel(n_fs, n_tp, *refs), out_shape=j...  140 us

profile of v8, /device:TPU:33, one launch (start us, length us, event | category | flops | bytes accessed | tf_op | source)
XLA Modules:
  0.0 141.6 jit_solution(7957057306438183198)
XLA Ops:
  0.0 139.9 %shard_map.127 = bf16[384,256]{1,0:T(8,128)(2,1)} custom-call(bf16[384,256]{1,0:T(8,128)(2,1)} %refs_0_.1, bf16[704,128]{1,0:T(8,128)(2,1)} %bitcast.2, bf16[704,128]{1,0:T(8,128)(2,1)} %bitcast.3, bf16[704,128]{1,0:T(8,128)(2,1)} %refs_3_.1, bf16[128,128]{1,0:T(8,128)(2,1)} %refs_4_.1, bf16[128,128]{1,0:T(8,128)(2,1)} %refs_5_.1, bf16[128,128]{1,0:T(8,128)(2,1)} %refs_6_.1, ...), custom_call_target="tpu_custom_call" | custom-call | tf_op jit(solution)/shard_map/pallas_call | solution.py:714
  140.0 1.6 %copy.15 = bf16[384,256]{1,0:T(8,128)(2,1)} copy(bf16[384,256]{1,0:T(8,128)(2,1)} %shard_map.127) | data formatting | bytes 393216

commit v9 on v7

--- a/solution.py
+++ b/solution.py
@@ -334,8 +334,11 @@
             rs_refs[n].at[(q, *src)], rs_refs[n].at[(q, *dst)], rs_send.at[n], rs_recv.at[2 * nq * n + q, i], where
         )
 
-    def sib_copy(n, q):
-        return rs_copy((slice(0, 4),), (slice(4, 8),), n, q, 0, sib)
+    def sib_first(n, q):
+        return rs_copy((0,), (4,), n, q, 0, sib)
+
+    def sib_rest(n, q):
+        return rs_copy((slice(1, 4),), (slice(5, 8),), n, q, 3, sib)
 
     def opp_copy(n, q, i):
         part = pl.ds(i * half, half)
@@ -349,21 +352,28 @@
         width_k = units if n == 0 else 2 * units
         k_range = pl.ds(pl.multiple_of(mine * units, LANES), units) if n == 0 else slice(None)
         h = hid[q * rows : (q + 1) * rows, 0:width_k]
+
+        def partial(k, side):
+            return jnp.dot(h, wd[2 * order[k] + side, k_range, :], preferred_element_type=F32)
+
+        buf[q, 0] = partial(0, other).astype(BF16)
+        sib_first(n, q).start()
+        for k in range(1, 4):
+            buf[q, k] = partial(k, other).astype(BF16)
+        sib_rest(n, q).start()
         for k in range(4):
-            buf[q, k] = jnp.dot(h, wd[2 * order[k] + other, k_range, :], preferred_element_type=F32).astype(BF16)
-        sib_copy(n, q).start()
-        for k in range(4):
-            acc[q, k] = jnp.dot(h, wd[2 * order[k] + core, k_range, :], preferred_element_type=F32)
+            acc[q, k] = partial(k, core)
 
     def rs_opposite(n, q):
         buf = rs_refs[n]
-        sib_copy(n, q).wait_recv()
+        sib_first(n, q).wait_recv()
         buf[q, 8] = (acc[q, 0] + buf[q, 4].astype(F32)).astype(BF16)
         opp_copy(n, q, 0).start()
         opp_copy(n, q, 1).start()
 
     def rs_neighbours(n, q):
         buf = rs_refs[n]
+        sib_rest(n, q).wait_recv()
         rs_copy((9,), (9,), n, q, 1, sib).wait_recv()
         for i in range(2):
             near, far = pl.ds(i * half, half), pl.ds((1 - i) * half, half)
@@ -741,7 +751,7 @@
                 dma((1,)),
                 dma((2 + 3 * nq, 3)),
                 dma((4,)),
-                dma((3 * nq, 3)),
+                dma((3 * nq, 4)),
                 dma((2,)),
                 dma((nq + 1,)),
                 dma((2,)),

time: 141 us -> 142 us (level)
  no operation moved by 1% of the time
where the time goes in v9:
time: 142 us
  Pallas kernels  140 us (99%)
  local copies, waits for them, and re-layouts  1.62 us (1%)
    pallas_call x1, Pallas kernels, local(): pl.pallas_call(lambda *refs: layer_kernel(n_fs, n_tp, *refs), out_shape=j...  140 us

profile of v9, /device:TPU:33, one launch (start us, length us, event | category | flops | bytes accessed | tf_op | source)
XLA Modules:
  0.0 141.6 jit_solution(4100380860129945736)
XLA Ops:
  0.0 139.9 %shard_map.127 = bf16[384,256]{1,0:T(8,128)(2,1)} custom-call(bf16[384,256]{1,0:T(8,128)(2,1)} %refs_0_.1, bf16[704,128]{1,0:T(8,128)(2,1)} %bitcast.2, bf16[704,128]{1,0:T(8,128)(2,1)} %bitcast.3, bf16[704,128]{1,0:T(8,128)(2,1)} %refs_3_.1, bf16[128,128]{1,0:T(8,128)(2,1)} %refs_4_.1, bf16[128,128]{1,0:T(8,128)(2,1)} %refs_5_.1, bf16[128,128]{1,0:T(8,128)(2,1)} %refs_6_.1, ...), custom_call_target="tpu_custom_call" | custom-call | tf_op jit(solution)/shard_map/pallas_call | solution.py:717
  140.0 1.6 %copy.15 = bf16[384,256]{1,0:T(8,128)(2,1)} copy(bf16[384,256]{1,0:T(8,128)(2,1)} %shard_map.127) | data formatting | bytes 393216
